TPU v7x, 32 devices: a whole 2x2x4 slice. The times are simulated.
32 devices in a mesh: sp: 8 (over z, x), tp: 4 (over y, core).
Axes of the slice: x: 2, y: 2, z: 4, core: 2. Of those that a mesh axis runs over, the one named last changes fastest.
Arguments:
- block_input: bfloat16 [2048, 2048], P('sp'), may hold values from -8 to 8
- queries: bfloat16 [2048, 1024], P('sp', 'tp'), may hold values from -6 to 6
- keys: bfloat16 [2048, 1024], P('sp', 'tp'), may hold values from -6 to 6
- w_value: bfloat16 [2048, 2048], P(None, 'tp'), may hold values from -0.125 to 0.125
- log_decay: float32 [2048, 1024], P('sp', 'tp'), as said below
- d_out: bfloat16 [2048, 2048], P('sp', 'tp'), may hold values from -0.125 to 0.125
Outputs:
- d_queries: bfloat16 [2048, 1024], P('sp', 'tp')
- d_keys: bfloat16 [2048, 1024], P('sp', 'tp')
- d_log_decay: float32 [2048, 1024], P('sp', 'tp')
- d_w_value: float32 [2048, 2048], P('sp', 'tp')
- row_norms: float32 [2048], P('sp')
Inputs may be any that keep to these rules, and one draw needn't show every extreme that they name: log_decay is negative; key channels differ in rate, and rates change along the sequence.
All inputs are finite; a program needn't handle non-finite values.
Results may differ from a plain program's by a relative error of at most 0.015.
Values sent between devices are 32-bit elements; how exact they have to be, the bound alone decides.
A program may use at most 64 MiB of HBM per device.

v0:
```python
import functools

import jax
import jax.numpy as jnp
from jax import lax
from jax.experimental import pallas as pl
from jax.experimental.pallas import tpu as pltpu
from jax.sharding import PartitionSpec as P

DK = 128
DV = 256
BLOCK = 32
F32 = jnp.float32
BF16 = jnp.bfloat16
MESH = pl.DeviceIdType.MESH


def nn(left, right):
    return lax.dot_general(left, right, (((1,), (0,)), ((), ())), preferred_element_type=F32)


def nt(left, right):
    return lax.dot_general(left, right, (((1,), (1,)), ((), ())), preferred_element_type=F32)


def tn(left, right):
    return lax.dot_general(left, right, (((0,), (0,)), ((), ())), preferred_element_type=F32)


def pieces(value, count):
    parts = []
    for _ in range(count):
        part = value.astype(BF16)
        parts.append(part)
        value = value - part.astype(F32)
    return parts


def ring_place(z, x, nz, nx):
    r = nz - 1 - z
    across = jnp.where(r % 2 == 0, x - 1, nx - 1 - x)
    return jnp.where(x == 0, z, nz + r * (nx - 1) + across)


def ring_member(p, nz, nx):
    u = jnp.maximum(p - nz, 0)
    r = u // (nx - 1)
    w = u % (nx - 1)
    x = jnp.where(r % 2 == 0, 1 + w, nx - 1 - w)
    return jnp.where(p < nz, p * nx, (nz - 1 - r) * nx + x)


def kernel(
    n, nx, ntp,
    x_hbm, q_hbm, k_hbm, w_hbm, g_hbm, o_hbm,
    dq_ref, dk_ref, dg_ref, dw_ref, rn_ref,
    x_ref, q_ref, k_ref, w_ref, g_ref, o_ref, in_sem,
    c_buf, span_buf, v_buf, qg_buf, kt_buf, ks_buf, y_buf, kp_buf, vp_buf, st_buf, xt_buf, vg_buf,
    a_out, a_in, z_out, z_in, z_acc, c_out, c_in, h_out, h_in, b_out, b_in, fr_buf,
    first, part, ring, norm_out, norm_in,
    a_send, a_recv, z_send, z_recv, c_send, c_recv, h_send, h_recv, b_send, b_recv, r_send, r_recv, n_send, n_recv,
):
    nz = n // nx
    me = lax.axis_index("sp")
    mine = lax.axis_index("tp")
    z, x = me // nx, me % nx
    tokens, heads = q_ref.shape[0], q_ref.shape[1] // DK
    blocks = tokens // BLOCK
    dvx = DV // nx
    scale = DK ** (-0.5)
    loads = [
        pltpu.make_async_copy(source, target, in_sem.at[i])
        for i, (source, target) in enumerate(
            [(g_hbm, g_ref), (q_hbm, q_ref), (o_hbm, o_ref), (k_hbm, k_ref), (x_hbm, x_ref), (w_hbm, w_ref)]
        )
    ]
    for load in loads:
        load.start()
    barrier = pltpu.get_barrier_semaphore()
    for off in range(1, nx):
        pl.semaphore_signal(
            barrier, inc=1, device_id={"sp": z * nx + (x + off) % nx}, device_id_type=MESH)
    for off in range(1, nz):
        pl.semaphore_signal(
            barrier, inc=1, device_id={"sp": (z + off) % nz * nx + x}, device_id_type=MESH)
    for off in range(1, ntp):
        pl.semaphore_signal(barrier, inc=1, device_id={"tp": (mine + off) % ntp}, device_id_type=MESH)

    row = lax.broadcasted_iota(jnp.int32, (tokens, tokens), 0)
    col = lax.broadcasted_iota(jnp.int32, (tokens, tokens), 1)
    below = col <= row
    inside = below & (col // BLOCK == row // BLOCK)
    tri = jnp.where(below, 1.0, 0.0).astype(BF16)
    tri_in = jnp.where(inside, 1.0, 0.0).astype(BF16)
    upper = jnp.where(col >= row, 1.0, 0.0).astype(BF16)
    last_in = jnp.where(col // BLOCK == row // BLOCK, 1.0, 0.0).astype(BF16)

    def hd(h):
        return slice(h * DK, (h + 1) * DK)

    def hv(h):
        return slice(h * DV, (h + 1) * DV)

    loads[0].wait()
    g_parts = pieces(g_ref[...], 3)
    span_buf[...] = sum(nn(tri, part_) for part_ in g_parts)
    c_buf[...] = sum(nn(tri_in, part_) for part_ in g_parts)
    total = span_buf[tokens - 1 : tokens, :]
    decay = jnp.exp(total)

    def scatter_copy(d, m, h):
        return pltpu.make_async_remote_copy(
            src_ref=a_out.at[d, m, h], dst_ref=a_in.at[d, x, h],
            send_sem=a_send.at[d, m, h], recv_sem=a_recv.at[d, x, h],
            device_id={"sp": z * nx + m}, device_id_type=MESH)

    def scatter_wait(d, h):
        for m in range(nx):
            @pl.when(m != x)
            def _():
                pltpu.make_async_remote_copy(
                    src_ref=a_out.at[d, m, h], dst_ref=a_in.at[d, m, h],
                    send_sem=a_send.at[d, m, h], recv_sem=a_recv.at[d, m, h],
                    device_id={"sp": z * nx + m}, device_id_type=MESH).wait_recv()

    def give(d, h, totals):
        for m in range(nx):
            a_out[d, m, h, :dvx, :] = totals[m * dvx : (m + 1) * dvx]
            a_out[d, m, h, dvx:, :] = jnp.broadcast_to(decay[:, hd(h)], (8, DK))
        for m in range(nx):
            @pl.when(m != x)
            def _():
                scatter_copy(d, m, h).start()

            @pl.when(m == x)
            def _():
                a_in[d, m, h] = a_out[d, m, h]

    loads[1].wait()
    q_all = q_ref[...].astype(F32) * scale
    q_span = (q_all * jnp.exp(span_buf[...])).astype(BF16)
    loads[2].wait()
    for h in range(heads):
        adjoint = tn(o_ref[:, hv(h)], q_span[:, hd(h)])
        if h == 0:
            pl.semaphore_wait(barrier, nx - 1 + nz - 1 + ntp - 1)
        give(1, h, adjoint)

    for load in loads[3:]:
        load.wait()
    k_all = k_ref[...].astype(F32)
    k_far = jnp.exp(total - span_buf[...])
    k_span = (k_all * k_far).astype(BF16)
    for h in range(heads):
        v_buf[:, hv(h)] = nn(x_ref[...], w_ref[:, hv(h)]).astype(BF16)
        give(0, h, tn(v_buf[:, hv(h)], k_span[:, hd(h)]))

    def order(d):
        return range(nx) if d == 0 else range(nx - 1, -1, -1)

    def plane_copy(dz):
        return pltpu.make_async_remote_copy(
            src_ref=z_out, dst_ref=z_in.at[z],
            send_sem=z_send.at[dz], recv_sem=z_recv.at[z],
            device_id={"sp": (z + dz) * nx + x}, device_id_type=MESH)

    def composite(d, h, rows_):
        acc, dec = None, None
        for m in order(d):
            local, rate = a_in[d, m, h, rows_, :], a_in[d, m, h, dvx : dvx + 1, :]
            acc = local if acc is None else local + rate * acc
            dec = rate if dec is None else rate * dec
        return acc, dec

    def forward_start():
        for h in range(heads):
            scatter_wait(0, h)
            acc, dec = composite(0, h, slice(0, dvx))
            z_out[h, :dvx, :] = acc
            z_out[h, dvx:, :] = jnp.broadcast_to(dec, (8, DK))
        for dz in range(1, nz):
            @pl.when(z + dz < nz)
            def _():
                plane_copy(dz).start()

    @pl.when(z < nz - 1)
    def _():
        forward_start()

    half_v = dvx // 4

    def chain_copy(c):
        return pltpu.make_async_remote_copy(
            src_ref=h_out.at[c], dst_ref=h_in.at[c],
            send_sem=h_send.at[c], recv_sem=h_recv.at[c],
            device_id={"sp": (z - 1) * nx + x}, device_id_type=MESH)

    def piece_copy(m, c):
        return pltpu.make_async_remote_copy(
            src_ref=b_out.at[m, c], dst_ref=b_in.at[x, c],
            send_sem=b_send.at[m, c], recv_sem=b_recv.at[x, c],
            device_id={"sp": z * nx + m}, device_id_type=MESH)

    for c in range(4 * heads):
        h, rows_ = c // 4, slice(c % 4 * half_v, (c % 4 + 1) * half_v)
        if c % 4 == 0:
            scatter_wait(1, h)
        acc, dec = composite(1, h, rows_)

        @pl.when(z == nz - 1)
        def _():
            h_in[c] = jnp.zeros((half_v, DK), F32)

        @pl.when(z < nz - 1)
        def _():
            chain_copy(c).wait_recv()

        enter = h_in[c]

        @pl.when(z > 0)
        def _():
            h_out[c] = acc + dec * enter
            chain_copy(c).start()

        for m in order(1):
            b_out[m, c] = enter
            enter = a_in[1, m, h, rows_, :] + a_in[1, m, h, dvx : dvx + 1, :] * enter
        for m in range(nx):
            @pl.when(m != x)
            def _():
                piece_copy(m, c).start()

            @pl.when(m == x)
            def _():
                b_in[m, c] = b_out[m, c]

    @pl.when(z == nz - 1)
    def _():
        for h in range(heads):
            scatter_wait(0, h)

    cum = c_buf[...]
    block_end = sum(nn(last_in, part_) for part_ in g_parts)
    k_tail = jnp.exp(block_end - cum)
    grow = jnp.exp(cum)
    qg_buf[...] = (q_all * grow).astype(BF16)
    ks_buf[...] = (k_all * jnp.exp(-cum)).astype(BF16)
    kt_buf[...] = (k_all * k_tail).astype(BF16)
    st_buf[...] = jnp.zeros_like(st_buf)

    def adjoint_step(step, carry):
        rows = pl.ds(pl.multiple_of((blocks - 1 - step) * BLOCK, BLOCK), BLOCK)
        for h in range(heads):
            keep = jnp.exp(c_buf[rows, hd(h)][BLOCK - 1 :])
            adjoint = st_buf[1, h]
            narrow = adjoint.astype(BF16)
            kp_buf[rows, hd(h)] = nn(v_buf[rows, hv(h)], narrow)
            vp_buf[rows, hv(h)] = nt(kt_buf[rows, hd(h)], narrow)
            st_buf[1, h] = keep * adjoint + tn(o_ref[rows, hv(h)], qg_buf[rows, hd(h)])
        return carry

    def state_step(step, carry):
        rows = pl.ds(pl.multiple_of(step * BLOCK, BLOCK), BLOCK)
        for h in range(heads):
            keep = jnp.exp(c_buf[rows, hd(h)][BLOCK - 1 :])
            state = st_buf[0, h]
            y_buf[rows, hd(h)] = nn(o_ref[rows, hv(h)], state.astype(BF16))
            st_buf[0, h] = keep * state + tn(v_buf[rows, hv(h)], kt_buf[rows, hd(h)])
        return carry

    lax.fori_loop(0, blocks, adjoint_step, 0)

    for h in range(heads):
        dots = jnp.where(inside, nt(qg_buf[:, hd(h)], ks_buf[:, hd(h)]), 0.0).astype(BF16)
        vp_buf[:, hv(h)] += tn(dots, o_ref[:, hv(h)])

    depth = x_ref.shape[1]
    for at in range(0, depth, 256):
        xt_buf[at : at + 256, :] = x_ref[:, at : at + 256].T

    def member_copy(m):
        return pltpu.make_async_remote_copy(
            src_ref=c_out.at[m], dst_ref=c_in.at[x],
            send_sem=c_send.at[m], recv_sem=c_recv.at[x],
            device_id={"sp": z * nx + m}, device_id_type=MESH)

    def forward_spread():
        z_acc[...] = jnp.zeros_like(z_acc)
        for zp in range(nz):
            @pl.when(zp < z)
            def _():
                pltpu.make_async_remote_copy(
                    src_ref=z_out, dst_ref=z_in.at[zp],
                    send_sem=z_send.at[0], recv_sem=z_recv.at[zp],
                    device_id={"sp": zp * nx + x}, device_id_type=MESH).wait_recv()
                for h in range(heads):
                    z_acc[h] = z_in[zp, h, :dvx, :] + z_in[zp, h, dvx : dvx + 1, :] * z_acc[h]
        for h in range(heads):
            acc = z_acc[h]
            for m in order(0):
                c_out[m, h] = acc
                acc = a_in[0, m, h, :dvx, :] + a_in[0, m, h, dvx : dvx + 1, :] * acc
        for m in range(nx):
            @pl.when(m != x)
            def _():
                member_copy(m).start()

            @pl.when(m == x)
            def _():
                c_in[m] = c_out[m]

    for h in range(heads):
        for m in range(nx):
            for c in range(4 * h, 4 * (h + 1)):
                @pl.when(m != x)
                def _():
                    pltpu.make_async_remote_copy(
                        src_ref=b_out.at[m, c], dst_ref=b_in.at[m, c],
                        send_sem=b_send.at[m, c], recv_sem=b_recv.at[m, c],
                        device_id={"sp": z * nx + m}, device_id_type=MESH).wait_recv()
                at = m * dvx + c % 4 * half_v
                fr_buf[h, at : at + half_v, :] = b_in[m, c]
        narrow = fr_buf[h].astype(BF16)
        vg_buf[:, hv(h)] = (vp_buf[:, hv(h)] + nt(k_span[:, hd(h)], narrow)).astype(BF16)

    own = dw_ref.shape[0]
    half_r, half_c = own // 2, dw_ref.shape[1] // 2
    p = ring_place(z, x, nz, nx)
    ahead = ring_member((p + 1) % n, nz, nx)
    behind = ring_member((p + n - 1) % n, nz, nx)

    def share(d, u, owner):
        rows_ = pl.ds(pl.multiple_of(owner * own + u * half_r, half_r), half_r)
        return nn(xt_buf[rows_, :], vg_buf[:, d * half_c : (d + 1) * half_c])

    def ring_copy(step, d, u, src):
        return pltpu.make_async_remote_copy(
            src_ref=src, dst_ref=ring.at[step, d, u],
            send_sem=r_send.at[step, d, u], recv_sem=r_recv.at[step, d, u],
            device_id={"sp": ahead if d == 0 else behind}, device_id_type=MESH)

    def owner_at(step, d):
        return ring_member((p + n - step - 1) % n if d == 0 else (p + step + 1) % n, nz, nx)

    for u in range(2):
        for d in range(2):
            first[d, u] = share(d, u, owner_at(0, d))
            ring_copy(0, d, u, first.at[d, u]).start()

    lax.fori_loop(0, blocks, state_step, 0)
    for h in range(heads):
        dots = jnp.where(inside, nt(o_ref[:, hv(h)], v_buf[:, hv(h)]), 0.0).astype(BF16)
        y_buf[:, hd(h)] += nn(dots, ks_buf[:, hd(h)])
        k_grad = (
            k_tail[:, hd(h)] * kp_buf[:, hd(h)]
            + jnp.exp(-cum[:, hd(h)]) * tn(dots, qg_buf[:, hd(h)])
            + k_far[:, hd(h)] * nn(v_buf[:, hv(h)], fr_buf[h].astype(BF16))
        )
        kp_buf[:, hd(h)] = k_grad
        dk_ref[:, hd(h)] = k_grad.astype(BF16)

    def query_side():
        for m in range(nx):
            @pl.when(m != x)
            def _():
                pltpu.make_async_remote_copy(
                    src_ref=c_out.at[m], dst_ref=c_in.at[m],
                    send_sem=c_send.at[m], recv_sem=c_recv.at[m],
                    device_id={"sp": z * nx + m}, device_id_type=MESH).wait_recv()
        for h in range(heads):
            state_in = jnp.concatenate([c_in[m, h] for m in range(nx)], axis=0)
            q_side = q_ref[:, hd(h)].astype(F32) * scale
            k_side = k_ref[:, hd(h)].astype(F32)
            q_grad = jnp.exp(c_buf[:, hd(h)]) * y_buf[:, hd(h)] + jnp.exp(span_buf[:, hd(h)]) * nn(
                o_ref[:, hv(h)], state_in.astype(BF16)
            )
            dq_ref[:, hd(h)] = (q_grad * scale).astype(BF16)
            terms = q_side * q_grad - k_side * kp_buf[:, hd(h)]
            far = jnp.exp(span_buf[tokens - 1 : tokens, hd(h)])
            span_end = st_buf[0, h] + far * state_in
            carry = jnp.sum(fr_buf[h] * span_end, axis=0, keepdims=True)
            dg_ref[:, hd(h)] = sum(nn(upper, part_) for part_ in pieces(terms, 3)) + carry

    def ring_step(step, carry):
        for d in range(2):
            for u in range(2):
                part[d, u] = share(d, u, owner_at(step, d))
        for u in range(2):
            for d in range(2):
                ring_copy(step - 1, d, u, first.at[d, u]).wait_recv()
                ring[step - 1, d, u] += part[d, u]
                ring_copy(step, d, u, ring.at[step - 1, d, u]).start()

        @pl.when(step == 2)
        def _():
            forward_spread()

        @pl.when(step == 4)
        def _():
            query_side()

        return carry

    lax.fori_loop(1, n - 1, ring_step, 0)

    for d in range(2):
        for u in range(2):
            part[d, u] = share(d, u, me)
    for u in range(2):
        squares = 0.0
        for d in range(2):
            ring_copy(n - 2, d, u, first.at[d, u]).wait_recv()
            done = ring[n - 2, d, u] + part[d, u]
            dw_ref[u * half_r : (u + 1) * half_r, d * half_c : (d + 1) * half_c] = done
            for at in range(0, half_c, 128):
                squares = squares + done[:, at : at + 128] * done[:, at : at + 128]
        norm_out[u] = jnp.broadcast_to(jnp.sum(squares.T, axis=0, keepdims=True), (8, half_r))

    def norm_copy(off):
        return pltpu.make_async_remote_copy(
            src_ref=norm_out, dst_ref=norm_in.at[off],
            send_sem=n_send.at[off], recv_sem=n_recv.at[off],
            device_id={"tp": (mine + off) % ntp}, device_id_type=MESH)

    for off in range(1, ntp):
        norm_copy(off).start()

    for m in range(nx):
        @pl.when(m != x)
        def _():
            for h in range(heads):
                for d in range(2):
                    scatter_copy(d, m, h).wait_send()
            for c in range(4 * heads):
                piece_copy(m, c).wait_send()
            member_copy(m).wait_send()
    for dz in range(1, nz):
        @pl.when(z + dz < nz)
        def _():
            plane_copy(dz).wait_send()

    @pl.when(z > 0)
    def _():
        for c in range(4 * heads):
            chain_copy(c).wait_send()

    def sent(step, carry):
        for u in range(2):
            for d in range(2):
                ring_copy(step, d, u, first.at[d, u]).wait_send()
        return carry

    lax.fori_loop(0, n - 1, sent, 0)
    norms = norm_out[...]
    for off in range(1, ntp):
        norm_copy(off).wait()
        norms = norms + norm_in[off]
    rn_ref[...] = norms


def finish(*refs):
    for source, target in zip(refs[:4], refs[5:9]):
        target[...] = source[...]
    refs[9][...] = refs[4][:, :1]


def on_device(n, nx, ntp, block_input, queries, keys, w_value, log_decay, d_out):
    tokens, wide = queries.shape
    heads = wide // DK
    cols = w_value.shape[1]
    depth = block_input.shape[1]
    own = depth // n
    nz = n // nx
    dvx = DV // nx
    vm = pltpu.VMEM
    dma = pltpu.SemaphoreType.DMA
    out = pl.pallas_call(
        functools.partial(kernel, n, nx, ntp),
        out_shape=(
            jax.ShapeDtypeStruct((tokens, wide), BF16),
            jax.ShapeDtypeStruct((tokens, wide), BF16),
            jax.ShapeDtypeStruct((tokens, wide), F32),
            jax.ShapeDtypeStruct((own, cols), F32),
            jax.ShapeDtypeStruct((2, 8, own // 2), F32),
        ),
        in_specs=[pl.BlockSpec(memory_space=pltpu.HBM)] * 6,
        out_specs=(pl.BlockSpec(memory_space=vm),) * 5,
        scratch_shapes=[
            vm(block_input.shape, BF16),
            vm(queries.shape, BF16),
            vm(keys.shape, BF16),
            vm(w_value.shape, BF16),
            vm(log_decay.shape, F32),
            vm(d_out.shape, BF16),
            dma((6,)),
            vm((tokens, wide), F32),
            vm((tokens, wide), F32),
            vm((tokens, cols), BF16),
            vm((tokens, wide), BF16),
            vm((tokens, wide), BF16),
            vm((tokens, wide), BF16),
            vm((tokens, wide), F32),
            vm((tokens, wide), F32),
            vm((tokens, cols), F32),
            vm((2, heads, DV, DK), F32),
            vm((depth, tokens), BF16),
            vm((tokens, cols), BF16),
            vm((2, nx, heads, dvx + 8, DK), F32),
            vm((2, nx, heads, dvx + 8, DK), F32),
            vm((heads, dvx + 8, DK), F32),
            vm((nz, heads, dvx + 8, DK), F32),
            vm((heads, dvx, DK), F32),
            vm((nx, heads, dvx, DK), F32),
            vm((nx, heads, dvx, DK), F32),
            vm((4 * heads, dvx // 4, DK), F32),
            vm((4 * heads, dvx // 4, DK), F32),
            vm((nx, 4 * heads, dvx // 4, DK), F32),
            vm((nx, 4 * heads, dvx // 4, DK), F32),
            vm((heads, DV, DK), F32),
            vm((2, 2, own // 2, cols // 2), F32),
            vm((2, 2, own // 2, cols // 2), F32),
            vm((n - 1, 2, 2, own // 2, cols // 2), F32),
            vm((2, 8, own // 2), F32),
            vm((ntp, 2, 8, own // 2), F32),
            dma((2, nx, heads)),
            dma((2, nx, heads)),
            dma((nz,)),
            dma((nz,)),
            dma((nx,)),
            dma((nx,)),
            dma((4 * heads,)),
            dma((4 * heads,)),
            dma((nx, 4 * heads)),
            dma((nx, 4 * heads)),
            dma((n - 1, 2, 2)),
            dma((n - 1, 2, 2)),
            dma((ntp,)),
            dma((ntp,)),
        ],
        compiler_params=pltpu.CompilerParams(
            collective_id=0, has_side_effects=True, vmem_limit_bytes=60 * 1024 * 1024
        ),
    )(block_input, queries, keys, w_value, log_decay, d_out)
    final = pl.pallas_call(
        finish,
        out_shape=tuple(jax.ShapeDtypeStruct(a.shape, a.dtype) for a in out[:4])
        + (jax.ShapeDtypeStruct((2, 1, own // 2), F32),),
        in_specs=[pl.BlockSpec(memory_space=vm)] * 5,
        out_specs=(pl.BlockSpec(memory_space=vm),) * 5,
        compiler_params=pltpu.CompilerParams(vmem_limit_bytes=60 * 1024 * 1024),
    )(*out)
    return (*final[:4], final[4].reshape(-1))


def solution(mesh):
    n, ntp = mesh.shape["sp"], mesh.shape["tp"]
    nx = 1 << ((n.bit_length() - 1) // 2)
    placed = (
        P("sp", None),
        P("sp", "tp"),
        P("sp", "tp"),
        P(None, "tp"),
        P("sp", "tp"),
        P("sp", "tp"),
    )
    return jax.shard_map(
        functools.partial(on_device, n, nx, ntp),
        mesh=mesh,
        in_specs=placed,
        out_specs=(P("sp", "tp"), P("sp", "tp"), P("sp", "tp"), P("sp", "tp"), P("sp")),
        check_vma=False,
    )
```

profile of v0, /device:TPU:0, one launch (start us, length us, event | category | flops | bytes accessed | tf_op | source)
XLA Modules:
  0.0 72.8 jit_solution(1677105697467997189)
XLA Ops:
  0.6 70.0 %shard_map.101 = (bf16[256,256]{1,0:T(8,128)(2,1)}, bf16[256,256]{1,0:T(8,128)(2,1)}, f32[256,256]{1,0:T(8,128)}, f32[256,512]{1,0:T(8,128)}, f32[2,8,128]{2,1,0:T(8,128)}) custom-call(bf16[256,2048]{1,0:T(8,128)(2,1)} %x_hbm.1, bf16[256,256]{1,0:T(8,128)(2,1)} %q_hbm.1, bf16[256,256]{1,0:T(8,128)(2,1)} %k_hbm.1, bf16[2048,512]{1,0:T(8,128)(2,1)} %w_hbm.1, ...), custom_call_target="tpu_custom_call" | custom-call | tf_op jit(solution)/shard_map/pallas_call | solution.py:477
  70.6 2.2 %shard_map.102 = (bf16[256,256]{1,0:T(8,128)(2,1)}, bf16[256,256]{1,0:T(8,128)(2,1)}, f32[256,256]{1,0:T(8,128)}, f32[256,512]{1,0:T(8,128)}, f32[2,1,128]{2,1,0:T(1,128)}) custom-call(bf16[256,256]{1,0:T(8,128)(2,1)} %get-tuple-element.15.refs_0_, bf16[256,256]{1,0:T(8,128)(2,1)} %get-tuple-element.16.refs_1_, f32[256,256]{1,0:T(8,128)} %get-tuple-element.17.refs_2_, ...), custom_call_target="tpu_custom_call" | custom-call | tf_op jit(solution)/shard_map/pallas_call | solution.py:544
where the time goes:
time: 73 us; the launch traced here: 72.8 us
  Pallas kernels  72.2 us (99%)
    pallas_call x1, Pallas kernels, on_device(): pl.pallas_call(functools.partial(kernel, n, nx, ntp), out_shape=(jax.Shap...  70 us
    pallas_call x1, Pallas kernels, on_device(): pl.pallas_call(finish, out_shape=tuple((jax.ShapeDtypeStruct(a.shape, a.d...  2.2 us

commit v1 on v0

--- a/solution.py
+++ b/solution.py
@@ -50,6 +50,10 @@
     return jnp.where(p < nz, p * nx, (nz - 1 - r) * nx + x)
 
 
+def is_cube(n, nx, ntp):
+    return nx == 2 and n == 4 * nx and ntp == 2 * nx
+
+
 def kernel(
     n, nx, ntp,
     x_hbm, q_hbm, k_hbm, w_hbm, g_hbm, o_hbm,
@@ -57,9 +61,16 @@
     x_ref, q_ref, k_ref, w_ref, g_ref, o_ref, in_sem,
     c_buf, span_buf, v_buf, qg_buf, kt_buf, ks_buf, y_buf, kp_buf, vp_buf, st_buf, xt_buf, vg_buf,
     a_out, a_in, z_out, z_in, z_acc, c_out, c_in, h_out, h_in, b_out, b_in, fr_buf,
-    first, part, ring, norm_out, norm_in,
-    a_send, a_recv, z_send, z_recv, c_send, c_recv, h_send, h_recv, b_send, b_recv, r_send, r_recv, n_send, n_recv,
+    norm_out, norm_in,
+    a_send, a_recv, z_send, z_recv, c_send, c_recv, h_send, h_recv, b_send, b_recv, n_send, n_recv,
+    *late,
 ):
+    cube = is_cube(n, nx, ntp)
+    if cube:
+        (xs_out, xr_in, xr_buf, vx_out, vx_in, vgp_buf, sx_out, sx_in, acc_buf, sm_out, sm_in,
+         xs_send, xr_recv, v_send, v_recv, sx_send, sx_recv, sm_send, sm_recv) = late
+    else:
+        first, part, ring, r_send, r_recv = late
     nz = n // nx
     me = lax.axis_index("sp")
     mine = lax.axis_index("tp")
@@ -146,8 +157,70 @@
             pl.semaphore_wait(barrier, nx - 1 + nz - 1 + ntp - 1)
         give(1, h, adjoint)
 
-    for load in loads[3:]:
-        load.wait()
+    loads[4].wait()
+    depth = x_ref.shape[1]
+    for at in range(0, depth, 256):
+        xt_buf[at : at + 256, :] = x_ref[:, at : at + 256].T
+
+    own = dw_ref.shape[0]
+    cols = dw_ref.shape[1]
+    wide = min(cols, 128)
+    chunks = cols // wide
+    half_r = own // 2
+    near, mirror = z + 1 - 2 * (z % 2), nz - 1 - z
+    core_mate, row_mate = mine + 1 - 2 * (mine % 2), (mine + 2) % 4
+
+    def gather_with(mode):
+        return near if mode == 0 else mirror
+
+    def scatter_with(mode):
+        return mirror if mode == 0 else near
+
+    def block_rows(slab, xx, base=0, size=None):
+        return pl.ds(pl.multiple_of((slab * nx + xx) * own + base, half_r), own if size is None else size)
+
+    def x_copy(mode):
+        return pltpu.make_async_remote_copy(
+            src_ref=xs_out.at[mode], dst_ref=xr_in.at[mode, mine],
+            send_sem=xs_send.at[mode, 0], recv_sem=xr_recv.at[mode, mine],
+            device_id={"sp": gather_with(mode) * nx + x}, device_id_type=MESH)
+
+    def x_pass(mode, which, block, mate):
+        return pltpu.make_async_remote_copy(
+            src_ref=xr_in.at[mode, block], dst_ref=xr_in.at[mode, block],
+            send_sem=xs_send.at[mode, which], recv_sem=xr_recv.at[mode, block],
+            device_id={"tp": mate}, device_id_type=MESH)
+
+    def x_send(mode):
+        slab = gather_with(mode)
+        other = nz - 1 - slab if mode == 0 else slab + 1 - 2 * (slab % 2)
+        slab = jnp.where(mine < nx, other, slab)
+        xs_out[mode] = xt_buf[block_rows(slab, mine % nx), :].astype(F32)
+        x_copy(mode).start()
+
+    def x_relay(mode):
+        x_copy(mode).wait_recv()
+        x_pass(mode, 1, mine, core_mate).start()
+        x_pass(mode, 2, mine, row_mate).start()
+
+    def x_forward(mode):
+        x_pass(mode, 2, row_mate, row_mate).wait_recv()
+        x_pass(mode, 3, row_mate, core_mate).start()
+
+    def x_take(mode):
+        x_pass(mode, 1, core_mate, core_mate).wait_recv()
+        far_mate = (core_mate + 2) % 4
+        x_pass(mode, 3, far_mate, core_mate).wait_recv()
+        for j in range(2 * nx):
+            xr_buf[mode, j] = xr_in[mode, j].astype(BF16)
+
+    if cube:
+        @pl.when(z < nz - 1)
+        def _():
+            x_send(0)
+
+    loads[3].wait()
+    loads[5].wait()
     k_all = k_ref[...].astype(F32)
     k_far = jnp.exp(total - span_buf[...])
     k_span = (k_all * k_far).astype(BF16)
@@ -183,9 +256,14 @@
             def _():
                 plane_copy(dz).start()
 
-    @pl.when(z < nz - 1)
+    @pl.when(z < nz - 2)
     def _():
         forward_start()
+
+    if cube:
+        @pl.when(z < nz - 2)
+        def _():
+            x_relay(0)
 
     half_v = dvx // 4
 
@@ -234,8 +312,14 @@
             def _():
                 b_in[m, c] = b_out[m, c]
 
+    @pl.when(z == nz - 2)
+    def _():
+        forward_start()
+
     @pl.when(z == nz - 1)
     def _():
+        if cube:
+            x_send(0)
         for h in range(heads):
             scatter_wait(0, h)
 
@@ -273,10 +357,6 @@
     for h in range(heads):
         dots = jnp.where(inside, nt(qg_buf[:, hd(h)], ks_buf[:, hd(h)]), 0.0).astype(BF16)
         vp_buf[:, hv(h)] += tn(dots, o_ref[:, hv(h)])
-
-    depth = x_ref.shape[1]
-    for at in range(0, depth, 256):
-        xt_buf[at : at + 256, :] = x_ref[:, at : at + 256].T
 
     def member_copy(m):
         return pltpu.make_async_remote_copy(
@@ -309,6 +389,53 @@
             def _():
                 c_in[m] = c_out[m]
 
+    modes = [0] * chunks
+
+    def near_copy(c):
+        return pltpu.make_async_remote_copy(
+            src_ref=vx_out.at[c], dst_ref=vx_in.at[c],
+            send_sem=v_send.at[c], recv_sem=v_recv.at[c],
+            device_id={"sp": gather_with(modes[c]) * nx + x}, device_id_type=MESH)
+
+    def side_copy(c, s, u):
+        return pltpu.make_async_remote_copy(
+            src_ref=sx_out.at[c, s, u], dst_ref=sx_in.at[c, s, u],
+            send_sem=sx_send.at[c, s, u], recv_sem=sx_recv.at[c, s, u],
+            device_id={"sp": z * nx + 1 - x}, device_id_type=MESH)
+
+    def far_copy(c, u):
+        return pltpu.make_async_remote_copy(
+            src_ref=sm_out.at[c, u], dst_ref=sm_in.at[c, u],
+            send_sem=sm_send.at[c, u], recv_sem=sm_recv.at[c, u],
+            device_id={"sp": scatter_with(modes[c]) * nx + x}, device_id_type=MESH)
+
+    def piece(c, s, xx):
+        at = slice(c * wide, (c + 1) * wide)
+        slab = scatter_with(modes[c]) if s == 0 else z
+        return nn(xt_buf[block_rows(slab, xx), :], vg_buf[:, at]) + nn(
+            xr_buf[modes[c], s * nx + xx], vgp_buf[:, at])
+
+    def take_near(c):
+        near_copy(c).wait_recv()
+        vgp_buf[:, c * wide : (c + 1) * wide] = vx_in[c].astype(BF16)
+
+    def side_send(c, s):
+        value = piece(c, s, 1 - x)
+        for u in range(2):
+            sx_out[c, s, u] = value[u * half_r : (u + 1) * half_r]
+            side_copy(c, s, u).start()
+
+    def keep(c, s):
+        value = piece(c, s, x)
+        for u in range(2):
+            acc_buf[c, s, u] = value[u * half_r : (u + 1) * half_r]
+
+    def far_send(c):
+        for u in range(2):
+            side_copy(c, 0, u).wait_recv()
+            sm_out[c, u] = acc_buf[c, 0, u] + sx_in[c, 0, u]
+            far_copy(c, u).start()
+
     for h in range(heads):
         for m in range(nx):
             for c in range(4 * h, 4 * (h + 1)):
@@ -322,9 +449,12 @@
                 fr_buf[h, at : at + half_v, :] = b_in[m, c]
         narrow = fr_buf[h].astype(BF16)
         vg_buf[:, hv(h)] = (vp_buf[:, hv(h)] + nt(k_span[:, hd(h)], narrow)).astype(BF16)
-
-    own = dw_ref.shape[0]
-    half_r, half_c = own // 2, dw_ref.shape[1] // 2
+        if cube:
+            for c in range(h * DV // wide, (h + 1) * DV // wide):
+                vx_out[c] = vg_buf[:, c * wide : (c + 1) * wide].astype(F32)
+                near_copy(c).start()
+
+    half_c = cols // 2
     p = ring_place(z, x, nz, nx)
     ahead = ring_member((p + 1) % n, nz, nx)
     behind = ring_member((p + n - 1) % n, nz, nx)
@@ -342,10 +472,21 @@
     def owner_at(step, d):
         return ring_member((p + n - step - 1) % n if d == 0 else (p + step + 1) % n, nz, nx)
 
-    for u in range(2):
-        for d in range(2):
-            first[d, u] = share(d, u, owner_at(0, d))
-            ring_copy(0, d, u, first.at[d, u]).start()
+    if not cube:
+        for u in range(2):
+            for d in range(2):
+                first[d, u] = share(d, u, owner_at(0, d))
+                ring_copy(0, d, u, first.at[d, u]).start()
+
+    else:
+        @pl.when(z >= nz - 2)
+        def _():
+            x_relay(0)
+
+        @pl.when(z < nz - 2)
+        def _():
+            x_forward(0)
+            forward_spread()
 
     lax.fori_loop(0, blocks, state_step, 0)
     for h in range(heads):
@@ -359,15 +500,18 @@
         kp_buf[:, hd(h)] = k_grad
         dk_ref[:, hd(h)] = k_grad.astype(BF16)
 
-    def query_side():
+    def query_side(first_head=0, last_head=heads):
         for m in range(nx):
+            if first_head:
+                break
+
             @pl.when(m != x)
             def _():
                 pltpu.make_async_remote_copy(
                     src_ref=c_out.at[m], dst_ref=c_in.at[m],
                     send_sem=c_send.at[m], recv_sem=c_recv.at[m],
                     device_id={"sp": z * nx + m}, device_id_type=MESH).wait_recv()
-        for h in range(heads):
+        for h in range(first_head, last_head):
             state_in = jnp.concatenate([c_in[m, h] for m in range(nx)], axis=0)
             q_side = q_ref[:, hd(h)].astype(F32) * scale
             k_side = k_ref[:, hd(h)].astype(F32)
@@ -401,20 +545,54 @@
 
         return carry
 
-    lax.fori_loop(1, n - 1, ring_step, 0)
-
-    for d in range(2):
+    if not cube:
+        lax.fori_loop(1, n - 1, ring_step, 0)
+
+        for d in range(2):
+            for u in range(2):
+                part[d, u] = share(d, u, me)
         for u in range(2):
-            part[d, u] = share(d, u, me)
-    for u in range(2):
-        squares = 0.0
-        for d in range(2):
-            ring_copy(n - 2, d, u, first.at[d, u]).wait_recv()
-            done = ring[n - 2, d, u] + part[d, u]
-            dw_ref[u * half_r : (u + 1) * half_r, d * half_c : (d + 1) * half_c] = done
-            for at in range(0, half_c, 128):
-                squares = squares + done[:, at : at + 128] * done[:, at : at + 128]
-        norm_out[u] = jnp.broadcast_to(jnp.sum(squares.T, axis=0, keepdims=True), (8, half_r))
+            squares = 0.0
+            for d in range(2):
+                ring_copy(n - 2, d, u, first.at[d, u]).wait_recv()
+                done = ring[n - 2, d, u] + part[d, u]
+                dw_ref[u * half_r : (u + 1) * half_r, d * half_c : (d + 1) * half_c] = done
+                for at in range(0, half_c, 128):
+                    squares = squares + done[:, at : at + 128] * done[:, at : at + 128]
+            norm_out[u] = jnp.broadcast_to(jnp.sum(squares.T, axis=0, keepdims=True), (8, half_r))
+    else:
+        @pl.when(z >= nz - 2)
+        def _():
+            x_forward(0)
+            forward_spread()
+
+        x_take(0)
+        take_near(0)
+        side_send(0, 0)
+        keep(0, 0)
+        side_send(0, 1)
+        keep(0, 1)
+        for c in range(1, chunks):
+            take_near(c)
+            side_send(c, 0)
+            keep(c, 0)
+            far_send(c - 1)
+            side_send(c, 1)
+            keep(c, 1)
+            if c == chunks - 2:
+                query_side(0, 1)
+        far_send(chunks - 1)
+        query_side(1, heads)
+        squares = [0.0, 0.0]
+        for c in range(chunks):
+            for u in range(2):
+                side_copy(c, 1, u).wait_recv()
+                far_copy(c, u).wait_recv()
+                done = acc_buf[c, 1, u] + sx_in[c, 1, u] + sm_in[c, u]
+                dw_ref[u * half_r : (u + 1) * half_r, c * wide : (c + 1) * wide] = done
+                squares[u] = squares[u] + done * done
+        for u in range(2):
+            norm_out[u] = jnp.broadcast_to(jnp.sum(squares[u].T, axis=0, keepdims=True), (8, half_r))
 
     def norm_copy(off):
         return pltpu.make_async_remote_copy(
@@ -444,13 +622,26 @@
         for c in range(4 * heads):
             chain_copy(c).wait_send()
 
-    def sent(step, carry):
-        for u in range(2):
-            for d in range(2):
-                ring_copy(step, d, u, first.at[d, u]).wait_send()
-        return carry
-
-    lax.fori_loop(0, n - 1, sent, 0)
+    if not cube:
+        def sent(step, carry):
+            for u in range(2):
+                for d in range(2):
+                    ring_copy(step, d, u, first.at[d, u]).wait_send()
+            return carry
+
+        lax.fori_loop(0, n - 1, sent, 0)
+    else:
+        x_copy(0).wait_send()
+        x_pass(0, 1, mine, core_mate).wait_send()
+        x_pass(0, 2, mine, row_mate).wait_send()
+        x_pass(0, 3, row_mate, core_mate).wait_send()
+        for c in range(chunks):
+            near_copy(c).wait_send()
+            for u in range(2):
+                side_copy(c, 0, u).wait_send()
+                side_copy(c, 1, u).wait_send()
+                far_copy(c, u).wait_send()
+
     norms = norm_out[...]
     for off in range(1, ntp):
         norm_copy(off).wait()
@@ -459,9 +650,13 @@
 
 
 def finish(*refs):
-    for source, target in zip(refs[:4], refs[5:9]):
-        target[...] = source[...]
+    sems = refs[10]
+    writes = [pltpu.make_async_copy(refs[i], refs[5 + i], sems.at[i]) for i in range(4)]
+    for write in writes:
+        write.start()
     refs[9][...] = refs[4][:, :1]
+    for write in writes:
+        write.wait()
 
 
 def on_device(n, nx, ntp, block_input, queries, keys, w_value, log_decay, d_out):
@@ -474,14 +669,45 @@
     dvx = DV // nx
     vm = pltpu.VMEM
     dma = pltpu.SemaphoreType.DMA
+    wide_c = min(cols, 128)
+    chunks, half = cols // wide_c, own // 2
+    late = [
+        vm((2, 2, half, cols // 2), F32),
+        vm((2, 2, half, cols // 2), F32),
+        vm((n - 1, 2, 2, half, cols // 2), F32),
+        dma((n - 1, 2, 2)),
+        dma((n - 1, 2, 2)),
+    ]
+    if is_cube(n, nx, ntp):
+        late = [
+            vm((2, own, tokens), F32),
+            vm((2, ntp, own, tokens), F32),
+            vm((2, ntp, own, tokens), BF16),
+            vm((chunks, tokens, wide_c), F32),
+            vm((chunks, tokens, wide_c), F32),
+            vm((tokens, cols), BF16),
+            vm((chunks, 2, 2, half, wide_c), F32),
+            vm((chunks, 2, 2, half, wide_c), F32),
+            vm((chunks, 2, 2, half, wide_c), F32),
+            vm((chunks, 2, half, wide_c), F32),
+            vm((chunks, 2, half, wide_c), F32),
+            dma((2, 4)),
+            dma((2, ntp)),
+            dma((chunks,)),
+            dma((chunks,)),
+            dma((chunks, 2, 2)),
+            dma((chunks, 2, 2)),
+            dma((chunks, 2)),
+            dma((chunks, 2)),
+        ]
     out = pl.pallas_call(
         functools.partial(kernel, n, nx, ntp),
         out_shape=(
-            jax.ShapeDtypeStruct((tokens, wide), BF16),
-            jax.ShapeDtypeStruct((tokens, wide), BF16),
-            jax.ShapeDtypeStruct((tokens, wide), F32),
-            jax.ShapeDtypeStruct((own, cols), F32),
-            jax.ShapeDtypeStruct((2, 8, own // 2), F32),
+            vm((tokens, wide), BF16),
+            vm((tokens, wide), BF16),
+            vm((tokens, wide), F32),
+            vm((own, cols), F32),
+            vm((2, 8, own // 2), F32),
         ),
         in_specs=[pl.BlockSpec(memory_space=pltpu.HBM)] * 6,
         out_specs=(pl.BlockSpec(memory_space=vm),) * 5,
@@ -517,9 +743,6 @@
             vm((nx, 4 * heads, dvx // 4, DK), F32),
             vm((nx, 4 * heads, dvx // 4, DK), F32),
             vm((heads, DV, DK), F32),
-            vm((2, 2, own // 2, cols // 2), F32),
-            vm((2, 2, own // 2, cols // 2), F32),
-            vm((n - 1, 2, 2, own // 2, cols // 2), F32),
             vm((2, 8, own // 2), F32),
             vm((ntp, 2, 8, own // 2), F32),
             dma((2, nx, heads)),
@@ -532,13 +755,12 @@
             dma((4 * heads,)),
             dma((nx, 4 * heads)),
             dma((nx, 4 * heads)),
-            dma((n - 1, 2, 2)),
-            dma((n - 1, 2, 2)),
             dma((ntp,)),
             dma((ntp,)),
+            *late,
         ],
         compiler_params=pltpu.CompilerParams(
-            collective_id=0, has_side_effects=True, vmem_limit_bytes=60 * 1024 * 1024
+            collective_id=0, has_side_effects=True, vmem_limit_bytes=62 * 1024 * 1024
         ),
     )(block_input, queries, keys, w_value, log_decay, d_out)
     final = pl.pallas_call(
@@ -546,8 +768,9 @@
         out_shape=tuple(jax.ShapeDtypeStruct(a.shape, a.dtype) for a in out[:4])
         + (jax.ShapeDtypeStruct((2, 1, own // 2), F32),),
         in_specs=[pl.BlockSpec(memory_space=vm)] * 5,
-        out_specs=(pl.BlockSpec(memory_space=vm),) * 5,
-        compiler_params=pltpu.CompilerParams(vmem_limit_bytes=60 * 1024 * 1024),
+        out_specs=(pl.BlockSpec(memory_space=pltpu.HBM),) * 4 + (pl.BlockSpec(memory_space=vm),),
+        scratch_shapes=[dma((4,))],
+        compiler_params=pltpu.CompilerParams(vmem_limit_bytes=1024 * 1024),
     )(*out)
     return (*final[:4], final[4].reshape(-1))
 

time: 73 us -> 59.9 us (0.82)
  Pallas kernels: 72.2 us -> 59.1 us
    pallas_call x1, Pallas kernels: 70 us -> 57.5 us  [on_device(): pl.pallas_call(functools.partial(kernel, n, nx, ntp), out_shape=(vm((toke...]
where the time goes in v1:
time: 59.9 us; the launch traced here: 59.7 us
  Pallas kernels  59.1 us (99%)
  between operations  0.64 us (1%)
    pallas_call x1, Pallas kernels, on_device(): pl.pallas_call(functools.partial(kernel, n, nx, ntp), out_shape=(vm((toke...  57.5 us
    pallas_call x1, Pallas kernels, on_device(): pl.pallas_call(finish, out_shape=tuple((jax.ShapeDtypeStruct(a.shape, a.d...  1.56 us

profile of v1, /device:TPU:0, one launch (start us, length us, event | category | flops | bytes accessed | tf_op | source)
XLA Modules:
  0.0 59.7 jit_solution(4058918211126455070)
XLA Ops:
  0.6 57.5 %shard_map.101 = (bf16[256,256]{1,0:T(8,128)(2,1)S(1)}, bf16[256,256]{1,0:T(8,128)(2,1)S(1)}, f32[256,256]{1,0:T(8,128)S(1)}, f32[256,512]{1,0:T(8,128)S(1)}, f32[2,8,128]{2,1,0:T(8,128)S(1)}) custom-call(bf16[256,2048]{1,0:T(8,128)(2,1)} %x_hbm.1, bf16[256,256]{1,0:T(8,128)(2,1)} %q_hbm.1, bf16[256,256]{1,0:T(8,128)(2,1)} %k_hbm.1, ...), custom_call_target="tpu_custom_call" | custom-call | tf_op jit(solution)/shard_map/pallas_call | solution.py:703
  58.2 1.6 %shard_map.102 = (bf16[256,256]{1,0:T(8,128)(2,1)}, bf16[256,256]{1,0:T(8,128)(2,1)}, f32[256,256]{1,0:T(8,128)}, f32[256,512]{1,0:T(8,128)}, f32[2,1,128]{2,1,0:T(1,128)}) custom-call(bf16[256,256]{1,0:T(8,128)(2,1)S(1)} %get-tuple-element.15.refs_0_, bf16[256,256]{1,0:T(8,128)(2,1)S(1)} %get-tuple-element.16.refs_1_, ...), custom_call_target="tpu_custom_call" | custom-call | tf_op jit(solution)/shard_map/pallas_call | solution.py:766

commit v2 on v1

--- a/solution.py
+++ b/solution.py
@@ -62,8 +62,8 @@
     c_buf, span_buf, v_buf, qg_buf, kt_buf, ks_buf, y_buf, kp_buf, vp_buf, st_buf, xt_buf, vg_buf,
     a_out, a_in, z_out, z_in, z_acc, c_out, c_in, h_out, h_in, b_out, b_in, fr_buf,
     norm_out, norm_in,
-    a_send, a_recv, z_send, z_recv, c_send, c_recv, h_send, h_recv, b_send, b_recv, n_send, n_recv,
-    *late,
+    a_send, a_recv, e_recv, z_send, z_recv, c_send, c_recv, h_send, h_recv, b_send, b_recv, n_send, n_recv,
+    tail_buf, *late,
 ):
     cube = is_cube(n, nx, ntp)
     if cube:
@@ -119,29 +119,56 @@
     total = span_buf[tokens - 1 : tokens, :]
     decay = jnp.exp(total)
 
-    def scatter_copy(d, m, h):
-        return pltpu.make_async_remote_copy(
-            src_ref=a_out.at[d, m, h], dst_ref=a_in.at[d, x, h],
-            send_sem=a_send.at[d, m, h], recv_sem=a_recv.at[d, x, h],
+    quarter = dvx // 4
+
+    def part_rows(part):
+        return slice(8 + part * quarter if part else 0, 8 + (part + 1) * quarter)
+
+    def slot(to, frm):
+        return (frm + nx - 1 - to) % nx
+
+    def first_part(m, h, part):
+        return pltpu.make_async_remote_copy(
+            src_ref=a_out.at[1, m, h, part_rows(part), :], dst_ref=a_in.at[1, x, h, part_rows(part), :],
+            send_sem=a_send.at[1, m], recv_sem=e_recv.at[slot(m, x), h * 4 + part],
             device_id={"sp": z * nx + m}, device_id_type=MESH)
 
-    def scatter_wait(d, h):
+    def first_wait(h, part):
         for m in range(nx):
             @pl.when(m != x)
             def _():
                 pltpu.make_async_remote_copy(
-                    src_ref=a_out.at[d, m, h], dst_ref=a_in.at[d, m, h],
-                    send_sem=a_send.at[d, m, h], recv_sem=a_recv.at[d, m, h],
+                    src_ref=a_out.at[1, m, h, part_rows(part), :], dst_ref=a_in.at[1, m, h, part_rows(part), :],
+                    send_sem=a_send.at[1, m], recv_sem=e_recv.at[slot(x, m), h * 4 + part],
+                    device_id={"sp": z * nx + m}, device_id_type=MESH).wait_recv()
+
+    def scatter_copy(d, m):
+        return pltpu.make_async_remote_copy(
+            src_ref=a_out.at[d, m], dst_ref=a_in.at[d, x],
+            send_sem=a_send.at[d, m], recv_sem=a_recv.at[slot(m, x)],
+            device_id={"sp": z * nx + m}, device_id_type=MESH)
+
+    def scatter_wait(d):
+        for m in range(nx):
+            @pl.when(m != x)
+            def _():
+                pltpu.make_async_remote_copy(
+                    src_ref=a_out.at[d, m], dst_ref=a_in.at[d, m],
+                    send_sem=a_send.at[d, m], recv_sem=a_recv.at[slot(x, m)],
                     device_id={"sp": z * nx + m}, device_id_type=MESH).wait_recv()
 
     def give(d, h, totals):
         for m in range(nx):
-            a_out[d, m, h, :dvx, :] = totals[m * dvx : (m + 1) * dvx]
-            a_out[d, m, h, dvx:, :] = jnp.broadcast_to(decay[:, hd(h)], (8, DK))
+            a_out[d, m, h, :8, :] = jnp.broadcast_to(decay[:, hd(h)], (8, DK))
+            a_out[d, m, h, 8:, :] = totals[m * dvx : (m + 1) * dvx]
         for m in range(nx):
             @pl.when(m != x)
             def _():
-                scatter_copy(d, m, h).start()
+                if d == 1:
+                    for part in range(4):
+                        first_part(m, h, part).start()
+                elif h == heads - 1:
+                    scatter_copy(d, m).start()
 
             @pl.when(m == x)
             def _():
@@ -170,54 +197,51 @@
     near, mirror = z + 1 - 2 * (z % 2), nz - 1 - z
     core_mate, row_mate = mine + 1 - 2 * (mine % 2), (mine + 2) % 4
 
-    def gather_with(mode):
-        return near if mode == 0 else mirror
-
-    def scatter_with(mode):
-        return mirror if mode == 0 else near
-
     def block_rows(slab, xx, base=0, size=None):
         return pl.ds(pl.multiple_of((slab * nx + xx) * own + base, half_r), own if size is None else size)
 
-    def x_copy(mode):
-        return pltpu.make_async_remote_copy(
-            src_ref=xs_out.at[mode], dst_ref=xr_in.at[mode, mine],
-            send_sem=xs_send.at[mode, 0], recv_sem=xr_recv.at[mode, mine],
-            device_id={"sp": gather_with(mode) * nx + x}, device_id_type=MESH)
-
-    def x_pass(mode, which, block, mate):
-        return pltpu.make_async_remote_copy(
-            src_ref=xr_in.at[mode, block], dst_ref=xr_in.at[mode, block],
-            send_sem=xs_send.at[mode, which], recv_sem=xr_recv.at[mode, block],
+    def x_copy(p):
+        return pltpu.make_async_remote_copy(
+            src_ref=xs_out.at[p], dst_ref=xr_in.at[mine, p],
+            send_sem=xs_send.at[0], recv_sem=xr_recv.at[mine, p],
+            device_id={"sp": near * nx + x}, device_id_type=MESH)
+
+    def x_pass(which, block, p, mate):
+        return pltpu.make_async_remote_copy(
+            src_ref=xr_in.at[block, p], dst_ref=xr_in.at[block, p],
+            send_sem=xs_send.at[which], recv_sem=xr_recv.at[block, p],
             device_id={"tp": mate}, device_id_type=MESH)
 
-    def x_send(mode):
-        slab = gather_with(mode)
-        other = nz - 1 - slab if mode == 0 else slab + 1 - 2 * (slab % 2)
-        slab = jnp.where(mine < nx, other, slab)
-        xs_out[mode] = xt_buf[block_rows(slab, mine % nx), :].astype(F32)
-        x_copy(mode).start()
-
-    def x_relay(mode):
-        x_copy(mode).wait_recv()
-        x_pass(mode, 1, mine, core_mate).start()
-        x_pass(mode, 2, mine, row_mate).start()
-
-    def x_forward(mode):
-        x_pass(mode, 2, row_mate, row_mate).wait_recv()
-        x_pass(mode, 3, row_mate, core_mate).start()
-
-    def x_take(mode):
-        x_pass(mode, 1, core_mate, core_mate).wait_recv()
+    def x_send(p):
+        slab = jnp.where(mine < nx, nz - 1 - near, near)
+        xs_out[p] = xt_buf[block_rows(slab, mine % nx, p * half_r, half_r), :].astype(F32)
+        x_copy(p).start()
+
+    def x_relay(p):
+        x_copy(p).wait_recv()
+        x_pass(2, mine, p, row_mate).start()
+        x_pass(1, mine, p, core_mate).start()
+
+    def x_forward():
+        for p in range(2):
+            x_pass(2, row_mate, p, row_mate).wait_recv()
+            x_pass(3, row_mate, p, core_mate).start()
+
+    def x_take():
         far_mate = (core_mate + 2) % 4
-        x_pass(mode, 3, far_mate, core_mate).wait_recv()
+        for p in range(2):
+            x_pass(1, core_mate, p, core_mate).wait_recv()
+            x_pass(3, far_mate, p, core_mate).wait_recv()
         for j in range(2 * nx):
-            xr_buf[mode, j] = xr_in[mode, j].astype(BF16)
+            for p in range(2):
+                xr_buf[j, p * half_r : (p + 1) * half_r] = xr_in[j, p].astype(BF16)
 
     if cube:
+        x_send(0)
+
         @pl.when(z < nz - 1)
         def _():
-            x_send(0)
+            x_send(1)
 
     loads[3].wait()
     loads[5].wait()
@@ -240,15 +264,15 @@
     def composite(d, h, rows_):
         acc, dec = None, None
         for m in order(d):
-            local, rate = a_in[d, m, h, rows_, :], a_in[d, m, h, dvx : dvx + 1, :]
+            local, rate = a_in[d, m, h, rows_, :], a_in[d, m, h, 0:1, :]
             acc = local if acc is None else local + rate * acc
             dec = rate if dec is None else rate * dec
         return acc, dec
 
     def forward_start():
+        scatter_wait(0)
         for h in range(heads):
-            scatter_wait(0, h)
-            acc, dec = composite(0, h, slice(0, dvx))
+            acc, dec = composite(0, h, slice(8, 8 + dvx))
             z_out[h, :dvx, :] = acc
             z_out[h, dvx:, :] = jnp.broadcast_to(dec, (8, DK))
         for dz in range(1, nz):
@@ -256,33 +280,68 @@
             def _():
                 plane_copy(dz).start()
 
+    def local_side():
+        cum = c_buf[...]
+        block_end = sum(nn(last_in, part_) for part_ in g_parts)
+        k_tail = jnp.exp(block_end - cum)
+        tail_buf[...] = k_tail
+        grow = jnp.exp(cum)
+        qg_buf[...] = (q_all * grow).astype(BF16)
+        ks_buf[...] = (k_all * jnp.exp(-cum)).astype(BF16)
+        kt_buf[...] = (k_all * k_tail).astype(BF16)
+        st_buf[...] = jnp.zeros_like(st_buf)
+
+        def adjoint_step(step, carry):
+            rows = pl.ds(pl.multiple_of((blocks - 1 - step) * BLOCK, BLOCK), BLOCK)
+            for h in range(heads):
+                keep = jnp.exp(c_buf[rows, hd(h)][BLOCK - 1 :])
+                adjoint = st_buf[1, h]
+                narrow = adjoint.astype(BF16)
+                kp_buf[rows, hd(h)] = nn(v_buf[rows, hv(h)], narrow)
+                vp_buf[rows, hv(h)] = nt(kt_buf[rows, hd(h)], narrow)
+                st_buf[1, h] = keep * adjoint + tn(o_ref[rows, hv(h)], qg_buf[rows, hd(h)])
+            return carry
+
+        lax.fori_loop(0, blocks, adjoint_step, 0)
+
+        for h in range(heads):
+            dots = jnp.where(inside, nt(qg_buf[:, hd(h)], ks_buf[:, hd(h)]), 0.0).astype(BF16)
+            vp_buf[:, hv(h)] += tn(dots, o_ref[:, hv(h)])
+
+    @pl.when(z < nz - 1)
+    def _():
+        local_side()
+
     @pl.when(z < nz - 2)
     def _():
         forward_start()
 
     if cube:
+        @pl.when(z < nz - 1)
+        def _():
+            x_relay(0)
+
         @pl.when(z < nz - 2)
         def _():
-            x_relay(0)
+            x_relay(1)
 
     half_v = dvx // 4
 
     def chain_copy(c):
         return pltpu.make_async_remote_copy(
             src_ref=h_out.at[c], dst_ref=h_in.at[c],
-            send_sem=h_send.at[c], recv_sem=h_recv.at[c],
+            send_sem=h_send, recv_sem=h_recv.at[c],
             device_id={"sp": (z - 1) * nx + x}, device_id_type=MESH)
 
     def piece_copy(m, c):
         return pltpu.make_async_remote_copy(
             src_ref=b_out.at[m, c], dst_ref=b_in.at[x, c],
-            send_sem=b_send.at[m, c], recv_sem=b_recv.at[x, c],
+            send_sem=b_send.at[m], recv_sem=b_recv.at[slot(m, x), c],
             device_id={"sp": z * nx + m}, device_id_type=MESH)
 
     for c in range(4 * heads):
-        h, rows_ = c // 4, slice(c % 4 * half_v, (c % 4 + 1) * half_v)
-        if c % 4 == 0:
-            scatter_wait(1, h)
+        h, rows_ = c // 4, slice(8 + c % 4 * half_v, 8 + (c % 4 + 1) * half_v)
+        first_wait(h, c % 4)
         acc, dec = composite(1, h, rows_)
 
         @pl.when(z == nz - 1)
@@ -302,7 +361,7 @@
 
         for m in order(1):
             b_out[m, c] = enter
-            enter = a_in[1, m, h, rows_, :] + a_in[1, m, h, dvx : dvx + 1, :] * enter
+            enter = a_in[1, m, h, rows_, :] + a_in[1, m, h, 0:1, :] * enter
         for m in range(nx):
             @pl.when(m != x)
             def _():
@@ -311,37 +370,13 @@
             @pl.when(m == x)
             def _():
                 b_in[m, c] = b_out[m, c]
-
-    @pl.when(z == nz - 2)
-    def _():
-        forward_start()
 
     @pl.when(z == nz - 1)
     def _():
         if cube:
-            x_send(0)
-        for h in range(heads):
-            scatter_wait(0, h)
-
-    cum = c_buf[...]
-    block_end = sum(nn(last_in, part_) for part_ in g_parts)
-    k_tail = jnp.exp(block_end - cum)
-    grow = jnp.exp(cum)
-    qg_buf[...] = (q_all * grow).astype(BF16)
-    ks_buf[...] = (k_all * jnp.exp(-cum)).astype(BF16)
-    kt_buf[...] = (k_all * k_tail).astype(BF16)
-    st_buf[...] = jnp.zeros_like(st_buf)
-
-    def adjoint_step(step, carry):
-        rows = pl.ds(pl.multiple_of((blocks - 1 - step) * BLOCK, BLOCK), BLOCK)
-        for h in range(heads):
-            keep = jnp.exp(c_buf[rows, hd(h)][BLOCK - 1 :])
-            adjoint = st_buf[1, h]
-            narrow = adjoint.astype(BF16)
-            kp_buf[rows, hd(h)] = nn(v_buf[rows, hv(h)], narrow)
-            vp_buf[rows, hv(h)] = nt(kt_buf[rows, hd(h)], narrow)
-            st_buf[1, h] = keep * adjoint + tn(o_ref[rows, hv(h)], qg_buf[rows, hd(h)])
-        return carry
+            x_send(1)
+        local_side()
+
 
     def state_step(step, carry):
         rows = pl.ds(pl.multiple_of(step * BLOCK, BLOCK), BLOCK)
@@ -351,12 +386,6 @@
             y_buf[rows, hd(h)] = nn(o_ref[rows, hv(h)], state.astype(BF16))
             st_buf[0, h] = keep * state + tn(v_buf[rows, hv(h)], kt_buf[rows, hd(h)])
         return carry
-
-    lax.fori_loop(0, blocks, adjoint_step, 0)
-
-    for h in range(heads):
-        dots = jnp.where(inside, nt(qg_buf[:, hd(h)], ks_buf[:, hd(h)]), 0.0).astype(BF16)
-        vp_buf[:, hv(h)] += tn(dots, o_ref[:, hv(h)])
 
     def member_copy(m):
         return pltpu.make_async_remote_copy(
@@ -379,7 +408,7 @@
             acc = z_acc[h]
             for m in order(0):
                 c_out[m, h] = acc
-                acc = a_in[0, m, h, :dvx, :] + a_in[0, m, h, dvx : dvx + 1, :] * acc
+                acc = a_in[0, m, h, 8:, :] + a_in[0, m, h, 0:1, :] * acc
         for m in range(nx):
             @pl.when(m != x)
             def _():
@@ -389,31 +418,29 @@
             def _():
                 c_in[m] = c_out[m]
 
-    modes = [0] * chunks
-
     def near_copy(c):
         return pltpu.make_async_remote_copy(
             src_ref=vx_out.at[c], dst_ref=vx_in.at[c],
-            send_sem=v_send.at[c], recv_sem=v_recv.at[c],
-            device_id={"sp": gather_with(modes[c]) * nx + x}, device_id_type=MESH)
+            send_sem=v_send, recv_sem=v_recv.at[c],
+            device_id={"sp": near * nx + x}, device_id_type=MESH)
 
     def side_copy(c, s, u):
         return pltpu.make_async_remote_copy(
             src_ref=sx_out.at[c, s, u], dst_ref=sx_in.at[c, s, u],
-            send_sem=sx_send.at[c, s, u], recv_sem=sx_recv.at[c, s, u],
+            send_sem=sx_send, recv_sem=sx_recv.at[c, s, u],
             device_id={"sp": z * nx + 1 - x}, device_id_type=MESH)
 
     def far_copy(c, u):
         return pltpu.make_async_remote_copy(
             src_ref=sm_out.at[c, u], dst_ref=sm_in.at[c, u],
-            send_sem=sm_send.at[c, u], recv_sem=sm_recv.at[c, u],
-            device_id={"sp": scatter_with(modes[c]) * nx + x}, device_id_type=MESH)
+            send_sem=sm_send, recv_sem=sm_recv.at[c, u],
+            device_id={"sp": mirror * nx + x}, device_id_type=MESH)
 
     def piece(c, s, xx):
         at = slice(c * wide, (c + 1) * wide)
-        slab = scatter_with(modes[c]) if s == 0 else z
+        slab = mirror if s == 0 else z
         return nn(xt_buf[block_rows(slab, xx), :], vg_buf[:, at]) + nn(
-            xr_buf[modes[c], s * nx + xx], vgp_buf[:, at])
+            xr_buf[s * nx + xx], vgp_buf[:, at])
 
     def take_near(c):
         near_copy(c).wait_recv()
@@ -443,7 +470,7 @@
                 def _():
                     pltpu.make_async_remote_copy(
                         src_ref=b_out.at[m, c], dst_ref=b_in.at[m, c],
-                        send_sem=b_send.at[m, c], recv_sem=b_recv.at[m, c],
+                        send_sem=b_send.at[m], recv_sem=b_recv.at[slot(x, m), c],
                         device_id={"sp": z * nx + m}, device_id_type=MESH).wait_recv()
                 at = m * dvx + c % 4 * half_v
                 fr_buf[h, at : at + half_v, :] = b_in[m, c]
@@ -478,14 +505,26 @@
                 first[d, u] = share(d, u, owner_at(0, d))
                 ring_copy(0, d, u, first.at[d, u]).start()
 
-    else:
+    @pl.when(z == nz - 2)
+    def _():
+        forward_start()
+
+    @pl.when(z == nz - 1)
+    def _():
+        scatter_wait(0)
+
+    if cube:
+        @pl.when(z == nz - 1)
+        def _():
+            x_relay(0)
+
         @pl.when(z >= nz - 2)
         def _():
-            x_relay(0)
+            x_relay(1)
 
         @pl.when(z < nz - 2)
         def _():
-            x_forward(0)
+            x_forward()
             forward_spread()
 
     lax.fori_loop(0, blocks, state_step, 0)
@@ -493,8 +532,8 @@
         dots = jnp.where(inside, nt(o_ref[:, hv(h)], v_buf[:, hv(h)]), 0.0).astype(BF16)
         y_buf[:, hd(h)] += nn(dots, ks_buf[:, hd(h)])
         k_grad = (
-            k_tail[:, hd(h)] * kp_buf[:, hd(h)]
-            + jnp.exp(-cum[:, hd(h)]) * tn(dots, qg_buf[:, hd(h)])
+            tail_buf[:, hd(h)] * kp_buf[:, hd(h)]
+            + jnp.exp(-c_buf[:, hd(h)]) * tn(dots, qg_buf[:, hd(h)])
             + k_far[:, hd(h)] * nn(v_buf[:, hv(h)], fr_buf[h].astype(BF16))
         )
         kp_buf[:, hd(h)] = k_grad
@@ -563,25 +602,27 @@
     else:
         @pl.when(z >= nz - 2)
         def _():
-            x_forward(0)
-            forward_spread()
-
-        x_take(0)
+            x_forward()
+
+        x_take()
         take_near(0)
         side_send(0, 0)
         keep(0, 0)
-        side_send(0, 1)
-        keep(0, 1)
         for c in range(1, chunks):
             take_near(c)
             side_send(c, 0)
+            side_send(c - 1, 1)
             keep(c, 0)
             far_send(c - 1)
-            side_send(c, 1)
-            keep(c, 1)
-            if c == chunks - 2:
-                query_side(0, 1)
+            keep(c - 1, 1)
+            if c == 2:
+                @pl.when(z >= nz - 2)
+                def _():
+                    forward_spread()
+        side_send(chunks - 1, 1)
+        query_side(0, 1)
         far_send(chunks - 1)
+        keep(chunks - 1, 1)
         query_side(1, heads)
         squares = [0.0, 0.0]
         for c in range(chunks):
@@ -606,11 +647,15 @@
     for m in range(nx):
         @pl.when(m != x)
         def _():
-            for h in range(heads):
-                for d in range(2):
-                    scatter_copy(d, m, h).wait_send()
-            for c in range(4 * heads):
-                piece_copy(m, c).wait_send()
+            for d in range(2):
+                pltpu.make_async_remote_copy(
+                    src_ref=a_out.at[d, m], dst_ref=a_in.at[d, x],
+                    send_sem=a_send.at[d, m], recv_sem=a_recv.at[slot(m, x)],
+                    device_id={"sp": z * nx + m}, device_id_type=MESH).wait_send()
+            pltpu.make_async_remote_copy(
+                src_ref=b_out.at[m], dst_ref=b_in.at[x],
+                send_sem=b_send.at[m], recv_sem=b_recv.at[slot(m, x), 0],
+                device_id={"sp": z * nx + m}, device_id_type=MESH).wait_send()
             member_copy(m).wait_send()
     for dz in range(1, nz):
         @pl.when(z + dz < nz)
@@ -619,8 +664,10 @@
 
     @pl.when(z > 0)
     def _():
-        for c in range(4 * heads):
-            chain_copy(c).wait_send()
+        pltpu.make_async_remote_copy(
+            src_ref=h_out, dst_ref=h_in,
+            send_sem=h_send, recv_sem=h_recv.at[0],
+            device_id={"sp": (z - 1) * nx + x}, device_id_type=MESH).wait_send()
 
     if not cube:
         def sent(step, carry):
@@ -631,16 +678,18 @@
 
         lax.fori_loop(0, n - 1, sent, 0)
     else:
-        x_copy(0).wait_send()
-        x_pass(0, 1, mine, core_mate).wait_send()
-        x_pass(0, 2, mine, row_mate).wait_send()
-        x_pass(0, 3, row_mate, core_mate).wait_send()
-        for c in range(chunks):
-            near_copy(c).wait_send()
-            for u in range(2):
-                side_copy(c, 0, u).wait_send()
-                side_copy(c, 1, u).wait_send()
-                far_copy(c, u).wait_send()
+        def all_sent(ref, sem):
+            pltpu.make_async_remote_copy(
+                src_ref=ref, dst_ref=ref, send_sem=sem, recv_sem=v_recv.at[0],
+                device_id={"sp": near * nx + x}, device_id_type=MESH).wait_send()
+
+        all_sent(xs_out, xs_send.at[0])
+        all_sent(xr_in.at[mine], xs_send.at[1])
+        all_sent(xr_in.at[mine], xs_send.at[2])
+        all_sent(xr_in.at[row_mate], xs_send.at[3])
+        all_sent(vx_out, v_send)
+        all_sent(sx_out, sx_send)
+        all_sent(sm_out, sm_send)
 
     norms = norm_out[...]
     for off in range(1, ntp):
@@ -680,9 +729,9 @@
     ]
     if is_cube(n, nx, ntp):
         late = [
-            vm((2, own, tokens), F32),
-            vm((2, ntp, own, tokens), F32),
-            vm((2, ntp, own, tokens), BF16),
+            vm((2, half, tokens), F32),
+            vm((ntp, 2, half, tokens), F32),
+            vm((ntp, own, tokens), BF16),
             vm((chunks, tokens, wide_c), F32),
             vm((chunks, tokens, wide_c), F32),
             vm((tokens, cols), BF16),
@@ -691,13 +740,13 @@
             vm((chunks, 2, 2, half, wide_c), F32),
             vm((chunks, 2, half, wide_c), F32),
             vm((chunks, 2, half, wide_c), F32),
-            dma((2, 4)),
-            dma((2, ntp)),
+            dma((4,)),
+            dma((ntp, 2)),
+            dma,
             dma((chunks,)),
-            dma((chunks,)),
+            dma,
             dma((chunks, 2, 2)),
-            dma((chunks, 2, 2)),
-            dma((chunks, 2)),
+            dma,
             dma((chunks, 2)),
         ]
     out = pl.pallas_call(
@@ -745,18 +794,20 @@
             vm((heads, DV, DK), F32),
             vm((2, 8, own // 2), F32),
             vm((ntp, 2, 8, own // 2), F32),
-            dma((2, nx, heads)),
-            dma((2, nx, heads)),
+            dma((2, nx)),
+            dma((nx - 1,)),
+            dma((nx - 1, 4 * heads)),
             dma((nz,)),
             dma((nz,)),
             dma((nx,)),
             dma((nx,)),
+            dma,
             dma((4 * heads,)),
-            dma((4 * heads,)),
-            dma((nx, 4 * heads)),
-            dma((nx, 4 * heads)),
+            dma((nx,)),
+            dma((nx - 1, 4 * heads)),
             dma((ntp,)),
             dma((ntp,)),
+            vm((tokens, wide), F32),
             *late,
         ],
         compiler_params=pltpu.CompilerParams(

time: 59.9 us -> 59.4 us (level)
  the two profiles are of different devices: /device:TPU:0 before, /device:TPU:17 now
where the time goes in v2:
time: 59.4 us; the launch traced here: 58.3 us
  Pallas kernels  57.6 us (97%)
  between operations  0.64 us (1%)
    pallas_call x1, Pallas kernels, on_device(): pl.pallas_call(functools.partial(kernel, n, nx, ntp), out_shape=(vm((toke...  56.1 us
    pallas_call x1, Pallas kernels, on_device(): pl.pallas_call(finish, out_shape=tuple((jax.ShapeDtypeStruct(a.shape, a.d...  1.56 us

profile of v2, /device:TPU:17, one launch (start us, length us, event | category | flops | bytes accessed | tf_op | source)
XLA Modules:
  0.0 58.3 jit_solution(13260619000484372228)
XLA Ops:
  0.6 56.1 %shard_map.101 = (bf16[256,256]{1,0:T(8,128)(2,1)S(1)}, bf16[256,256]{1,0:T(8,128)(2,1)S(1)}, f32[256,256]{1,0:T(8,128)S(1)}, f32[256,512]{1,0:T(8,128)S(1)}, f32[2,8,128]{2,1,0:T(8,128)S(1)}) custom-call(bf16[256,2048]{1,0:T(8,128)(2,1)} %x_hbm.1, bf16[256,256]{1,0:T(8,128)(2,1)} %q_hbm.1, bf16[256,256]{1,0:T(8,128)(2,1)} %k_hbm.1, ...), custom_call_target="tpu_custom_call" | custom-call | tf_op jit(solution)/shard_map/pallas_call | solution.py:752
  56.7 1.6 %shard_map.102 = (bf16[256,256]{1,0:T(8,128)(2,1)}, bf16[256,256]{1,0:T(8,128)(2,1)}, f32[256,256]{1,0:T(8,128)}, f32[256,512]{1,0:T(8,128)}, f32[2,1,128]{2,1,0:T(1,128)}) custom-call(bf16[256,256]{1,0:T(8,128)(2,1)S(1)} %get-tuple-element.15.refs_0_, bf16[256,256]{1,0:T(8,128)(2,1)S(1)} %get-tuple-element.16.refs_1_, ...), custom_call_target="tpu_custom_call" | custom-call | tf_op jit(solution)/shard_map/pallas_call | solution.py:817

commit v3 on v2

--- a/solution.py
+++ b/solution.py
@@ -65,7 +65,7 @@
     a_send, a_recv, e_recv, z_send, z_recv, c_send, c_recv, h_send, h_recv, b_send, b_recv, n_send, n_recv,
     tail_buf, *late,
 ):
-    cube = is_cube(n, nx, ntp)
+    cube = is_cube(n, nx, ntp) and dw_ref.shape[1] == 2 * DV
     if cube:
         (xs_out, xr_in, xr_buf, vx_out, vx_in, vgp_buf, sx_out, sx_in, acc_buf, sm_out, sm_in,
          xs_send, xr_recv, v_send, v_recv, sx_send, sx_recv, sm_send, sm_recv) = late
@@ -99,12 +99,10 @@
 
     row = lax.broadcasted_iota(jnp.int32, (tokens, tokens), 0)
     col = lax.broadcasted_iota(jnp.int32, (tokens, tokens), 1)
-    below = col <= row
-    inside = below & (col // BLOCK == row // BLOCK)
-    tri = jnp.where(below, 1.0, 0.0).astype(BF16)
-    tri_in = jnp.where(inside, 1.0, 0.0).astype(BF16)
-    upper = jnp.where(col >= row, 1.0, 0.0).astype(BF16)
-    last_in = jnp.where(col // BLOCK == row // BLOCK, 1.0, 0.0).astype(BF16)
+    tri = jnp.where(col <= row, 1.0, 0.0).astype(BF16)
+
+    def inside():
+        return (col <= row) & (col // BLOCK == row // BLOCK)
 
     def hd(h):
         return slice(h * DK, (h + 1) * DK)
@@ -115,7 +113,6 @@
     loads[0].wait()
     g_parts = pieces(g_ref[...], 3)
     span_buf[...] = sum(nn(tri, part_) for part_ in g_parts)
-    c_buf[...] = sum(nn(tri_in, part_) for part_ in g_parts)
     total = span_buf[tokens - 1 : tokens, :]
     decay = jnp.exp(total)
 
@@ -281,7 +278,10 @@
                 plane_copy(dz).start()
 
     def local_side():
-        cum = c_buf[...]
+        tri_in = jnp.where(inside(), 1.0, 0.0).astype(BF16)
+        last_in = jnp.where(col // BLOCK == row // BLOCK, 1.0, 0.0).astype(BF16)
+        cum = sum(nn(tri_in, part_) for part_ in g_parts)
+        c_buf[...] = cum
         block_end = sum(nn(last_in, part_) for part_ in g_parts)
         k_tail = jnp.exp(block_end - cum)
         tail_buf[...] = k_tail
@@ -305,78 +305,8 @@
         lax.fori_loop(0, blocks, adjoint_step, 0)
 
         for h in range(heads):
-            dots = jnp.where(inside, nt(qg_buf[:, hd(h)], ks_buf[:, hd(h)]), 0.0).astype(BF16)
+            dots = jnp.where(inside(), nt(qg_buf[:, hd(h)], ks_buf[:, hd(h)]), 0.0).astype(BF16)
             vp_buf[:, hv(h)] += tn(dots, o_ref[:, hv(h)])
-
-    @pl.when(z < nz - 1)
-    def _():
-        local_side()
-
-    @pl.when(z < nz - 2)
-    def _():
-        forward_start()
-
-    if cube:
-        @pl.when(z < nz - 1)
-        def _():
-            x_relay(0)
-
-        @pl.when(z < nz - 2)
-        def _():
-            x_relay(1)
-
-    half_v = dvx // 4
-
-    def chain_copy(c):
-        return pltpu.make_async_remote_copy(
-            src_ref=h_out.at[c], dst_ref=h_in.at[c],
-            send_sem=h_send, recv_sem=h_recv.at[c],
-            device_id={"sp": (z - 1) * nx + x}, device_id_type=MESH)
-
-    def piece_copy(m, c):
-        return pltpu.make_async_remote_copy(
-            src_ref=b_out.at[m, c], dst_ref=b_in.at[x, c],
-            send_sem=b_send.at[m], recv_sem=b_recv.at[slot(m, x), c],
-            device_id={"sp": z * nx + m}, device_id_type=MESH)
-
-    for c in range(4 * heads):
-        h, rows_ = c // 4, slice(8 + c % 4 * half_v, 8 + (c % 4 + 1) * half_v)
-        first_wait(h, c % 4)
-        acc, dec = composite(1, h, rows_)
-
-        @pl.when(z == nz - 1)
-        def _():
-            h_in[c] = jnp.zeros((half_v, DK), F32)
-
-        @pl.when(z < nz - 1)
-        def _():
-            chain_copy(c).wait_recv()
-
-        enter = h_in[c]
-
-        @pl.when(z > 0)
-        def _():
-            h_out[c] = acc + dec * enter
-            chain_copy(c).start()
-
-        for m in order(1):
-            b_out[m, c] = enter
-            enter = a_in[1, m, h, rows_, :] + a_in[1, m, h, 0:1, :] * enter
-        for m in range(nx):
-            @pl.when(m != x)
-            def _():
-                piece_copy(m, c).start()
-
-            @pl.when(m == x)
-            def _():
-                b_in[m, c] = b_out[m, c]
-
-    @pl.when(z == nz - 1)
-    def _():
-        if cube:
-            x_send(1)
-        local_side()
-
 
     def state_step(step, carry):
         rows = pl.ds(pl.multiple_of(step * BLOCK, BLOCK), BLOCK)
@@ -436,15 +366,22 @@
             send_sem=sm_send, recv_sem=sm_recv.at[c, u],
             device_id={"sp": mirror * nx + x}, device_id_type=MESH)
 
+    def emit(h, m):
+        c = h * nx + m
+        held = b_in[m, 4 * h : 4 * h + 4].reshape(dvx, DK).astype(BF16)
+        at = pl.ds(pl.multiple_of(c * wide, wide), wide)
+        value = (vp_buf[:, at] + nt(k_span[:, hd(h)], held)).astype(BF16)
+        vg_buf[c] = value
+        vx_out[c] = value.astype(F32)
+        near_copy(c).start()
+
     def piece(c, s, xx):
-        at = slice(c * wide, (c + 1) * wide)
         slab = mirror if s == 0 else z
-        return nn(xt_buf[block_rows(slab, xx), :], vg_buf[:, at]) + nn(
-            xr_buf[s * nx + xx], vgp_buf[:, at])
+        return nn(xt_buf[block_rows(slab, xx), :], vg_buf[c]) + nn(xr_buf[s * nx + xx], vgp_buf[c])
 
     def take_near(c):
         near_copy(c).wait_recv()
-        vgp_buf[:, c * wide : (c + 1) * wide] = vx_in[c].astype(BF16)
+        vgp_buf[c] = vx_in[c].astype(BF16)
 
     def side_send(c, s):
         value = piece(c, s, 1 - x)
@@ -463,23 +400,139 @@
             sm_out[c, u] = acc_buf[c, 0, u] + sx_in[c, 0, u]
             far_copy(c, u).start()
 
-    for h in range(heads):
+    @pl.when(z < nz - 1)
+    def _():
+        local_side()
+
+    if cube:
+        @pl.when(z < nz - 1)
+        def _():
+            x_relay(0)
+
+    @pl.when(z < nz - 2)
+    def _():
+        forward_start()
+
+    if cube:
+        @pl.when(z < nz - 2)
+        def _():
+            x_relay(1)
+
+        @pl.when(z == 0)
+        def _():
+            forward_spread()
+
+    half_v = dvx // 4
+
+    def chain_copy(c):
+        return pltpu.make_async_remote_copy(
+            src_ref=h_out.at[c], dst_ref=h_in.at[c],
+            send_sem=h_send, recv_sem=h_recv.at[c],
+            device_id={"sp": (z - 1) * nx + x}, device_id_type=MESH)
+
+    def piece_copy(m, c):
+        return pltpu.make_async_remote_copy(
+            src_ref=b_out.at[m, c], dst_ref=b_in.at[x, c],
+            send_sem=b_send.at[m], recv_sem=b_recv.at[slot(m, x), c],
+            device_id={"sp": z * nx + m}, device_id_type=MESH)
+
+    for c in range(4 * heads):
+        h, rows_ = c // 4, slice(8 + c % 4 * half_v, 8 + (c % 4 + 1) * half_v)
+        first_wait(h, c % 4)
+        acc, dec = composite(1, h, rows_)
+
+        @pl.when(z == nz - 1)
+        def _():
+            h_in[c] = jnp.zeros((half_v, DK), F32)
+
+        @pl.when(z < nz - 1)
+        def _():
+            chain_copy(c).wait_recv()
+
+        enter = h_in[c]
+
+        @pl.when(z > 0)
+        def _():
+            h_out[c] = acc + dec * enter
+            chain_copy(c).start()
+
+        for m in order(1):
+            b_out[m, c] = enter
+            enter = a_in[1, m, h, rows_, :] + a_in[1, m, h, 0:1, :] * enter
         for m in range(nx):
+            @pl.when(m != x)
+            def _():
+                piece_copy(m, c).start()
+
+            @pl.when(m == x)
+            def _():
+                b_in[m, c] = b_out[m, c]
+
+        if cube and c % 4 == 3:
+            @pl.when(z < nz - 1)
+            def _():
+                emit(h, x)
+
+    @pl.when(z == nz - 2)
+    def _():
+        forward_start()
+
+    @pl.when(z == nz - 1)
+    def _():
+        if cube:
+            x_send(1)
+        local_side()
+        if cube:
+            for h in range(heads):
+                emit(h, x)
+        scatter_wait(0)
+
+    def state_loop():
+        lax.fori_loop(0, blocks, state_step, 0)
+
+    if cube:
+        @pl.when((z > 0) & (z < nz - 2))
+        def _():
+            forward_spread()
+
+        state_loop()
+
+        @pl.when(z < nz - 2)
+        def _():
+            x_forward()
+
+        @pl.when(z == nz - 1)
+        def _():
+            x_relay(0)
+
+        @pl.when(z >= nz - 2)
+        def _():
+            x_relay(1)
+
+        for h in range(heads):
             for c in range(4 * h, 4 * (h + 1)):
-                @pl.when(m != x)
-                def _():
-                    pltpu.make_async_remote_copy(
-                        src_ref=b_out.at[m, c], dst_ref=b_in.at[m, c],
-                        send_sem=b_send.at[m], recv_sem=b_recv.at[slot(x, m), c],
-                        device_id={"sp": z * nx + m}, device_id_type=MESH).wait_recv()
-                at = m * dvx + c % 4 * half_v
-                fr_buf[h, at : at + half_v, :] = b_in[m, c]
-        narrow = fr_buf[h].astype(BF16)
-        vg_buf[:, hv(h)] = (vp_buf[:, hv(h)] + nt(k_span[:, hd(h)], narrow)).astype(BF16)
-        if cube:
-            for c in range(h * DV // wide, (h + 1) * DV // wide):
-                vx_out[c] = vg_buf[:, c * wide : (c + 1) * wide].astype(F32)
-                near_copy(c).start()
+                pltpu.make_async_remote_copy(
+                    src_ref=b_out.at[1 - x, c], dst_ref=b_in.at[1 - x, c],
+                    send_sem=b_send.at[1 - x], recv_sem=b_recv.at[0, c],
+                    device_id={"sp": z * nx + 1 - x}, device_id_type=MESH).wait_recv()
+            emit(h, 1 - x)
+            for m in range(nx):
+                fr_buf[h, m * dvx : (m + 1) * dvx, :] = b_in[m, 4 * h : 4 * h + 4].reshape(dvx, DK)
+    else:
+        for h in range(heads):
+            for m in range(nx):
+                for c in range(4 * h, 4 * (h + 1)):
+                    @pl.when(m != x)
+                    def _():
+                        pltpu.make_async_remote_copy(
+                            src_ref=b_out.at[m, c], dst_ref=b_in.at[m, c],
+                            send_sem=b_send.at[m], recv_sem=b_recv.at[slot(x, m), c],
+                            device_id={"sp": z * nx + m}, device_id_type=MESH).wait_recv()
+                    at = m * dvx + c % 4 * half_v
+                    fr_buf[h, at : at + half_v, :] = b_in[m, c]
+            narrow = fr_buf[h].astype(BF16)
+            vg_buf[:, hv(h)] = (vp_buf[:, hv(h)] + nt(k_span[:, hd(h)], narrow)).astype(BF16)
+
 
     half_c = cols // 2
     p = ring_place(z, x, nz, nx)
@@ -505,39 +558,21 @@
                 first[d, u] = share(d, u, owner_at(0, d))
                 ring_copy(0, d, u, first.at[d, u]).start()
 
-    @pl.when(z == nz - 2)
-    def _():
-        forward_start()
-
-    @pl.when(z == nz - 1)
-    def _():
-        scatter_wait(0)
-
-    if cube:
-        @pl.when(z == nz - 1)
-        def _():
-            x_relay(0)
-
-        @pl.when(z >= nz - 2)
-        def _():
-            x_relay(1)
-
-        @pl.when(z < nz - 2)
-        def _():
-            x_forward()
-            forward_spread()
-
-    lax.fori_loop(0, blocks, state_step, 0)
-    for h in range(heads):
-        dots = jnp.where(inside, nt(o_ref[:, hv(h)], v_buf[:, hv(h)]), 0.0).astype(BF16)
-        y_buf[:, hd(h)] += nn(dots, ks_buf[:, hd(h)])
-        k_grad = (
-            tail_buf[:, hd(h)] * kp_buf[:, hd(h)]
-            + jnp.exp(-c_buf[:, hd(h)]) * tn(dots, qg_buf[:, hd(h)])
-            + k_far[:, hd(h)] * nn(v_buf[:, hv(h)], fr_buf[h].astype(BF16))
-        )
-        kp_buf[:, hd(h)] = k_grad
-        dk_ref[:, hd(h)] = k_grad.astype(BF16)
+    def key_side():
+        for h in range(heads):
+            dots = jnp.where(inside(), nt(o_ref[:, hv(h)], v_buf[:, hv(h)]), 0.0).astype(BF16)
+            y_buf[:, hd(h)] += nn(dots, ks_buf[:, hd(h)])
+            k_grad = (
+                tail_buf[:, hd(h)] * kp_buf[:, hd(h)]
+                + jnp.exp(-c_buf[:, hd(h)]) * tn(dots, qg_buf[:, hd(h)])
+                + k_far[:, hd(h)] * nn(v_buf[:, hv(h)], fr_buf[h].astype(BF16))
+            )
+            kp_buf[:, hd(h)] = k_grad
+            dk_ref[:, hd(h)] = k_grad.astype(BF16)
+
+    if not cube:
+        state_loop()
+        key_side()
 
     def query_side(first_head=0, last_head=heads):
         for m in range(nx):
@@ -550,6 +585,7 @@
                     src_ref=c_out.at[m], dst_ref=c_in.at[m],
                     send_sem=c_send.at[m], recv_sem=c_recv.at[m],
                     device_id={"sp": z * nx + m}, device_id_type=MESH).wait_recv()
+        upper = jnp.where(col >= row, 1.0, 0.0).astype(BF16)
         for h in range(first_head, last_head):
             state_in = jnp.concatenate([c_in[m, h] for m in range(nx)], axis=0)
             q_side = q_ref[:, hd(h)].astype(F32) * scale
@@ -604,33 +640,48 @@
         def _():
             x_forward()
 
+        k0, k1, k2, k3 = x, nx + x, 1 - x, nx + 1 - x
         x_take()
-        take_near(0)
-        side_send(0, 0)
-        keep(0, 0)
-        for c in range(1, chunks):
-            take_near(c)
-            side_send(c, 0)
-            side_send(c - 1, 1)
-            keep(c, 0)
-            far_send(c - 1)
-            keep(c - 1, 1)
-            if c == 2:
-                @pl.when(z >= nz - 2)
-                def _():
-                    forward_spread()
-        side_send(chunks - 1, 1)
+        take_near(k0)
+        side_send(k0, 0)
+        take_near(k1)
+        side_send(k1, 0)
+        side_send(k0, 1)
+        key_side()
+        take_near(k2)
+        side_send(k2, 0)
+        keep(k2, 0)
+        far_send(k2)
+        side_send(k1, 1)
+        take_near(k3)
+        side_send(k3, 0)
+        keep(k3, 0)
+        far_send(k3)
+        side_send(k2, 1)
+        keep(k0, 0)
+        keep(k1, 0)
+
+        @pl.when(z >= nz - 2)
+        def _():
+            forward_spread()
+
+        far_send(k0)
+        side_send(k3, 1)
+        keep(k2, 1)
+        keep(k3, 1)
         query_side(0, 1)
-        far_send(chunks - 1)
-        keep(chunks - 1, 1)
+        far_send(k1)
+        keep(k0, 1)
+        keep(k1, 1)
         query_side(1, heads)
         squares = [0.0, 0.0]
-        for c in range(chunks):
+        for c in (k2, k3, k0, k1):
+            at = pl.ds(pl.multiple_of(c * wide, wide), wide)
             for u in range(2):
                 side_copy(c, 1, u).wait_recv()
                 far_copy(c, u).wait_recv()
                 done = acc_buf[c, 1, u] + sx_in[c, 1, u] + sm_in[c, u]
-                dw_ref[u * half_r : (u + 1) * half_r, c * wide : (c + 1) * wide] = done
+                dw_ref[u * half_r : (u + 1) * half_r, at] = done
                 squares[u] = squares[u] + done * done
         for u in range(2):
             norm_out[u] = jnp.broadcast_to(jnp.sum(squares[u].T, axis=0, keepdims=True), (8, half_r))
@@ -727,14 +778,15 @@
         dma((n - 1, 2, 2)),
         dma((n - 1, 2, 2)),
     ]
-    if is_cube(n, nx, ntp):
+    cube = is_cube(n, nx, ntp) and cols == 2 * DV
+    if cube:
         late = [
             vm((2, half, tokens), F32),
             vm((ntp, 2, half, tokens), F32),
             vm((ntp, own, tokens), BF16),
             vm((chunks, tokens, wide_c), F32),
             vm((chunks, tokens, wide_c), F32),
-            vm((tokens, cols), BF16),
+            vm((chunks, tokens, wide_c), BF16),
             vm((chunks, 2, 2, half, wide_c), F32),
             vm((chunks, 2, 2, half, wide_c), F32),
             vm((chunks, 2, 2, half, wide_c), F32),
@@ -779,7 +831,7 @@
             vm((tokens, cols), F32),
             vm((2, heads, DV, DK), F32),
             vm((depth, tokens), BF16),
-            vm((tokens, cols), BF16),
+            vm((chunks, tokens, wide_c) if cube else (tokens, cols), BF16),
             vm((2, nx, heads, dvx + 8, DK), F32),
             vm((2, nx, heads, dvx + 8, DK), F32),
             vm((heads, dvx + 8, DK), F32),

time: 59.4 us -> 60.1 us (1.012); the launches traced: 58.3 us -> 59.9 us
  Pallas kernels: 57.6 us -> 59.3 us
    pallas_call x1, Pallas kernels: 56.1 us -> 57.7 us  [on_device(): pl.pallas_call(functools.partial(kernel, n, nx, ntp), out_shape=(vm((toke...]
where the time goes in v3:
time: 60.1 us; the launch traced here: 59.9 us
  Pallas kernels  59.3 us (99%)
  between operations  0.64 us (1%)
    pallas_call x1, Pallas kernels, on_device(): pl.pallas_call(functools.partial(kernel, n, nx, ntp), out_shape=(vm((toke...  57.7 us
    pallas_call x1, Pallas kernels, on_device(): pl.pallas_call(finish, out_shape=tuple((jax.ShapeDtypeStruct(a.shape, a.d...  1.56 us

profile of v3, /device:TPU:17, one launch (start us, length us, event | category | flops | bytes accessed | tf_op | source)
XLA Modules:
  0.0 59.9 jit_solution(10775183150457434598)
XLA Ops:
  0.6 57.7 %shard_map.101 = (bf16[256,256]{1,0:T(8,128)(2,1)S(1)}, bf16[256,256]{1,0:T(8,128)(2,1)S(1)}, f32[256,256]{1,0:T(8,128)S(1)}, f32[256,512]{1,0:T(8,128)S(1)}, f32[2,8,128]{2,1,0:T(8,128)S(1)}) custom-call(bf16[256,2048]{1,0:T(8,128)(2,1)} %x_hbm.1, bf16[256,256]{1,0:T(8,128)(2,1)} %q_hbm.1, bf16[256,256]{1,0:T(8,128)(2,1)} %k_hbm.1, ...), custom_call_target="tpu_custom_call" | custom-call | tf_op jit(solution)/shard_map/pallas_call | solution.py:804
  58.4 1.6 %shard_map.102 = (bf16[256,256]{1,0:T(8,128)(2,1)}, bf16[256,256]{1,0:T(8,128)(2,1)}, f32[256,256]{1,0:T(8,128)}, f32[256,512]{1,0:T(8,128)}, f32[2,1,128]{2,1,0:T(1,128)}) custom-call(bf16[256,256]{1,0:T(8,128)(2,1)S(1)} %get-tuple-element.15.refs_0_, bf16[256,256]{1,0:T(8,128)(2,1)S(1)} %get-tuple-element.16.refs_1_, ...), custom_call_target="tpu_custom_call" | custom-call | tf_op jit(solution)/shard_map/pallas_call | solution.py:869

commit v4 on v3

--- a/solution.py
+++ b/solution.py
@@ -348,6 +348,44 @@
             def _():
                 c_in[m] = c_out[m]
 
+    def step_copy():
+        return pltpu.make_async_remote_copy(
+            src_ref=z_out, dst_ref=z_in.at[0],
+            send_sem=z_send.at[0], recv_sem=z_recv.at[0],
+            device_id={"sp": (z + 1) * nx + x}, device_id_type=MESH)
+
+    def forward_step():
+        @pl.when(z == 0)
+        def _():
+            z_acc[...] = jnp.zeros_like(z_acc)
+
+        @pl.when(z > 0)
+        def _():
+            step_copy().wait_recv()
+            for h in range(heads):
+                z_acc[h] = z_in[0, h, :dvx, :]
+
+        for h in range(heads):
+            acc = z_acc[h]
+            for m in order(0):
+                c_out[m, h] = acc
+                acc = a_in[0, m, h, 8:, :] + a_in[0, m, h, 0:1, :] * acc
+            z_out[h, :dvx, :] = acc
+            z_out[h, dvx:, :] = jnp.zeros((8, DK), F32)
+
+        @pl.when(z < nz - 1)
+        def _():
+            step_copy().start()
+
+        for m in range(nx):
+            @pl.when(m != x)
+            def _():
+                member_copy(m).start()
+
+            @pl.when(m == x)
+            def _():
+                c_in[m] = c_out[m]
+
     def near_copy(c):
         return pltpu.make_async_remote_copy(
             src_ref=vx_out.at[c], dst_ref=vx_in.at[c],
@@ -409,9 +447,10 @@
         def _():
             x_relay(0)
 
-    @pl.when(z < nz - 2)
-    def _():
-        forward_start()
+    if not cube:
+        @pl.when(z < nz - 2)
+        def _():
+            forward_start()
 
     if cube:
         @pl.when(z < nz - 2)
@@ -420,7 +459,8 @@
 
         @pl.when(z == 0)
         def _():
-            forward_spread()
+            scatter_wait(0)
+            forward_step()
 
     half_v = dvx // 4
 
@@ -469,13 +509,19 @@
                 b_in[m, c] = b_out[m, c]
 
         if cube and c % 4 == 3:
-            @pl.when(z < nz - 1)
+            @pl.when((z < nz - 1) & (z % 2 == 0))
             def _():
                 emit(h, x)
 
-    @pl.when(z == nz - 2)
-    def _():
-        forward_start()
+    if cube:
+        @pl.when((z < nz - 1) & (z % 2 == 1))
+        def _():
+            for h in range(heads):
+                emit(h, x)
+    else:
+        @pl.when(z == nz - 2)
+        def _():
+            forward_start()
 
     @pl.when(z == nz - 1)
     def _():
@@ -483,27 +529,21 @@
             x_send(1)
         local_side()
         if cube:
+            x_relay(0)
             for h in range(heads):
                 emit(h, x)
-        scatter_wait(0)
+        else:
+            scatter_wait(0)
 
     def state_loop():
         lax.fori_loop(0, blocks, state_step, 0)
 
     if cube:
-        @pl.when((z > 0) & (z < nz - 2))
-        def _():
-            forward_spread()
-
         state_loop()
 
         @pl.when(z < nz - 2)
         def _():
             x_forward()
-
-        @pl.when(z == nz - 1)
-        def _():
-            x_relay(0)
 
         @pl.when(z >= nz - 2)
         def _():
@@ -640,40 +680,52 @@
         def _():
             x_forward()
 
+        @pl.when((z > 0) & (z < nz - 2))
+        def _():
+            scatter_wait(0)
+            forward_step()
+
         k0, k1, k2, k3 = x, nx + x, 1 - x, nx + 1 - x
         x_take()
         take_near(k0)
         side_send(k0, 0)
         take_near(k1)
         side_send(k1, 0)
-        side_send(k0, 1)
         key_side()
         take_near(k2)
         side_send(k2, 0)
+
+        @pl.when(z == nz - 2)
+        def _():
+            scatter_wait(0)
+            forward_step()
+
         keep(k2, 0)
         far_send(k2)
-        side_send(k1, 1)
+        side_send(k0, 1)
         take_near(k3)
         side_send(k3, 0)
         keep(k3, 0)
         far_send(k3)
-        side_send(k2, 1)
+        side_send(k1, 1)
         keep(k0, 0)
         keep(k1, 0)
 
-        @pl.when(z >= nz - 2)
-        def _():
-            forward_spread()
-
+        side_send(k2, 1)
         far_send(k0)
         side_send(k3, 1)
+
+        @pl.when(z == nz - 1)
+        def _():
+            scatter_wait(0)
+            forward_step()
+
         keep(k2, 1)
         keep(k3, 1)
-        query_side(0, 1)
         far_send(k1)
         keep(k0, 1)
         keep(k1, 1)
-        query_side(1, heads)
+        query_side(0, heads)
         squares = [0.0, 0.0]
         for c in (k2, k3, k0, k1):
             at = pl.ds(pl.multiple_of(c * wide, wide), wide)
@@ -708,10 +760,15 @@
                 send_sem=b_send.at[m], recv_sem=b_recv.at[slot(m, x), 0],
                 device_id={"sp": z * nx + m}, device_id_type=MESH).wait_send()
             member_copy(m).wait_send()
-    for dz in range(1, nz):
-        @pl.when(z + dz < nz)
-        def _():
-            plane_copy(dz).wait_send()
+    if cube:
+        @pl.when(z < nz - 1)
+        def _():
+            step_copy().wait_send()
+    else:
+        for dz in range(1, nz):
+            @pl.when(z + dz < nz)
+            def _():
+                plane_copy(dz).wait_send()
 
     @pl.when(z > 0)
     def _():

time: 60.1 us -> 55.3 us (0.920)
  the two profiles are of different devices: /device:TPU:17 before, /device:TPU:0 now
where the time goes in v4:
time: 55.3 us; the launch traced here: 55.2 us
  Pallas kernels  54.5 us (99%)
  between operations  0.64 us (1%)
    pallas_call x1, Pallas kernels, on_device(): pl.pallas_call(functools.partial(kernel, n, nx, ntp), out_shape=(vm((toke...  53 us
    pallas_call x1, Pallas kernels, on_device(): pl.pallas_call(finish, out_shape=tuple((jax.ShapeDtypeStruct(a.shape, a.d...  1.56 us

profile of v4, /device:TPU:0, one launch (start us, length us, event | category | flops | bytes accessed | tf_op | source)
XLA Modules:
  0.0 55.2 jit_solution(2843870699407344414)
XLA Ops:
  0.6 53.0 %shard_map.101 = (bf16[256,256]{1,0:T(8,128)(2,1)S(1)}, bf16[256,256]{1,0:T(8,128)(2,1)S(1)}, f32[256,256]{1,0:T(8,128)S(1)}, f32[256,512]{1,0:T(8,128)S(1)}, f32[2,8,128]{2,1,0:T(8,128)S(1)}) custom-call(bf16[256,2048]{1,0:T(8,128)(2,1)} %x_hbm.1, bf16[256,256]{1,0:T(8,128)(2,1)} %q_hbm.1, bf16[256,256]{1,0:T(8,128)(2,1)} %k_hbm.1, ...), custom_call_target="tpu_custom_call" | custom-call | tf_op jit(solution)/shard_map/pallas_call | solution.py:861
  53.6 1.6 %shard_map.102 = (bf16[256,256]{1,0:T(8,128)(2,1)}, bf16[256,256]{1,0:T(8,128)(2,1)}, f32[256,256]{1,0:T(8,128)}, f32[256,512]{1,0:T(8,128)}, f32[2,1,128]{2,1,0:T(1,128)}) custom-call(bf16[256,256]{1,0:T(8,128)(2,1)S(1)} %get-tuple-element.15.refs_0_, bf16[256,256]{1,0:T(8,128)(2,1)S(1)} %get-tuple-element.16.refs_1_, ...), custom_call_target="tpu_custom_call" | custom-call | tf_op jit(solution)/shard_map/pallas_call | solution.py:926

commit v5 on v4

--- a/solution.py
+++ b/solution.py
@@ -63,12 +63,12 @@
     a_out, a_in, z_out, z_in, z_acc, c_out, c_in, h_out, h_in, b_out, b_in, fr_buf,
     norm_out, norm_in,
     a_send, a_recv, e_recv, z_send, z_recv, c_send, c_recv, h_send, h_recv, b_send, b_recv, n_send, n_recv,
-    tail_buf, *late,
+    tail_buf, ksp_buf, *late,
 ):
     cube = is_cube(n, nx, ntp) and dw_ref.shape[1] == 2 * DV
     if cube:
         (xs_out, xr_in, xr_buf, vx_out, vx_in, vgp_buf, sx_out, sx_in, acc_buf, sm_out, sm_in,
-         xs_send, xr_recv, v_send, v_recv, sx_send, sx_recv, sm_send, sm_recv) = late
+         xs_send, xr_recv, xc_recv, v_send, v_recv, sx_send, sx_recv, sm_send, sm_recv) = late
     else:
         first, part, ring, r_send, r_recv = late
     nz = n // nx
@@ -110,11 +110,8 @@
     def hv(h):
         return slice(h * DV, (h + 1) * DV)
 
-    loads[0].wait()
-    g_parts = pieces(g_ref[...], 3)
-    span_buf[...] = sum(nn(tri, part_) for part_ in g_parts)
-    total = span_buf[tokens - 1 : tokens, :]
-    decay = jnp.exp(total)
+    def total(h):
+        return span_buf[tokens - 1 : tokens, hd(h)]
 
     quarter = dvx // 4
 
@@ -156,7 +153,7 @@
 
     def give(d, h, totals):
         for m in range(nx):
-            a_out[d, m, h, :8, :] = jnp.broadcast_to(decay[:, hd(h)], (8, DK))
+            a_out[d, m, h, :8, :] = jnp.broadcast_to(jnp.exp(total(h)), (8, DK))
             a_out[d, m, h, 8:, :] = totals[m * dvx : (m + 1) * dvx]
         for m in range(nx):
             @pl.when(m != x)
@@ -171,12 +168,16 @@
             def _():
                 a_in[d, m, h] = a_out[d, m, h]
 
-    loads[1].wait()
-    q_all = q_ref[...].astype(F32) * scale
-    q_span = (q_all * jnp.exp(span_buf[...])).astype(BF16)
-    loads[2].wait()
+    loads[0].wait()
     for h in range(heads):
-        adjoint = tn(o_ref[:, hv(h)], q_span[:, hd(h)])
+        span = sum(nn(tri, part_) for part_ in pieces(g_ref[:, hd(h)], 3))
+        span_buf[:, hd(h)] = span
+        if h == 0:
+            loads[1].wait()
+        q_span = (q_ref[:, hd(h)].astype(F32) * scale * jnp.exp(span)).astype(BF16)
+        if h == 0:
+            loads[2].wait()
+        adjoint = tn(o_ref[:, hv(h)], q_span)
         if h == 0:
             pl.semaphore_wait(barrier, nx - 1 + nz - 1 + ntp - 1)
         give(1, h, adjoint)
@@ -195,23 +196,27 @@
     core_mate, row_mate = mine + 1 - 2 * (mine % 2), (mine + 2) % 4
 
     def block_rows(slab, xx, base=0, size=None):
-        return pl.ds(pl.multiple_of((slab * nx + xx) * own + base, half_r), own if size is None else size)
+        unit = half_r // 2
+        return pl.ds(pl.multiple_of((slab * nx + xx) * own + base, unit), own if size is None else size)
+
+    x_parts = 4
+    x_rows = own // x_parts
 
     def x_copy(p):
         return pltpu.make_async_remote_copy(
             src_ref=xs_out.at[p], dst_ref=xr_in.at[mine, p],
-            send_sem=xs_send.at[0], recv_sem=xr_recv.at[mine, p],
+            send_sem=xs_send.at[0], recv_sem=xr_recv.at[4 + p],
             device_id={"sp": near * nx + x}, device_id_type=MESH)
 
     def x_pass(which, block, p, mate):
         return pltpu.make_async_remote_copy(
             src_ref=xr_in.at[block, p], dst_ref=xr_in.at[block, p],
-            send_sem=xs_send.at[which], recv_sem=xr_recv.at[block, p],
+            send_sem=xs_send.at[which], recv_sem=xr_recv.at[p] if which == 2 else xc_recv.at[which // 2],
             device_id={"tp": mate}, device_id_type=MESH)
 
     def x_send(p):
         slab = jnp.where(mine < nx, nz - 1 - near, near)
-        xs_out[p] = xt_buf[block_rows(slab, mine % nx, p * half_r, half_r), :].astype(F32)
+        xs_out[p] = xt_buf[block_rows(slab, mine % nx, p * x_rows, x_rows), :].astype(F32)
         x_copy(p).start()
 
     def x_relay(p):
@@ -220,34 +225,38 @@
         x_pass(1, mine, p, core_mate).start()
 
     def x_forward():
-        for p in range(2):
+        for p in range(x_parts):
             x_pass(2, row_mate, p, row_mate).wait_recv()
             x_pass(3, row_mate, p, core_mate).start()
 
     def x_take():
         far_mate = (core_mate + 2) % 4
-        for p in range(2):
-            x_pass(1, core_mate, p, core_mate).wait_recv()
-            x_pass(3, far_mate, p, core_mate).wait_recv()
+        for i, block in enumerate((core_mate, far_mate)):
+            pltpu.make_async_remote_copy(
+                src_ref=xr_in.at[block], dst_ref=xr_in.at[block],
+                send_sem=xs_send.at[1], recv_sem=xc_recv.at[i],
+                device_id={"tp": core_mate}, device_id_type=MESH).wait_recv()
         for j in range(2 * nx):
-            for p in range(2):
-                xr_buf[j, p * half_r : (p + 1) * half_r] = xr_in[j, p].astype(BF16)
+            for p in range(x_parts):
+                xr_buf[j, p * x_rows : (p + 1) * x_rows] = xr_in[j, p].astype(BF16)
 
     if cube:
         x_send(0)
 
         @pl.when(z < nz - 1)
         def _():
-            x_send(1)
+            for p in range(1, x_parts):
+                x_send(p)
 
     loads[3].wait()
     loads[5].wait()
-    k_all = k_ref[...].astype(F32)
-    k_far = jnp.exp(total - span_buf[...])
-    k_span = (k_all * k_far).astype(BF16)
-    for h in range(heads):
-        v_buf[:, hv(h)] = nn(x_ref[...], w_ref[:, hv(h)]).astype(BF16)
-        give(0, h, tn(v_buf[:, hv(h)], k_span[:, hd(h)]))
+
+    def value_side(first_head=0, last_head=heads):
+        for h in range(first_head, last_head):
+            k_far = jnp.exp(total(h) - span_buf[:, hd(h)])
+            ksp_buf[:, hd(h)] = (k_ref[:, hd(h)].astype(F32) * k_far).astype(BF16)
+            v_buf[:, hv(h)] = nn(x_ref[...], w_ref[:, hv(h)]).astype(BF16)
+            give(0, h, tn(v_buf[:, hv(h)], ksp_buf[:, hd(h)]))
 
     def order(d):
         return range(nx) if d == 0 else range(nx - 1, -1, -1)
@@ -279,6 +288,9 @@
 
     def local_side():
         tri_in = jnp.where(inside(), 1.0, 0.0).astype(BF16)
+        g_parts = pieces(g_ref[...], 3)
+        q_all = q_ref[...].astype(F32) * scale
+        k_all = k_ref[...].astype(F32)
         last_in = jnp.where(col // BLOCK == row // BLOCK, 1.0, 0.0).astype(BF16)
         cum = sum(nn(tri_in, part_) for part_ in g_parts)
         c_buf[...] = cum
@@ -320,7 +332,7 @@
     def member_copy(m):
         return pltpu.make_async_remote_copy(
             src_ref=c_out.at[m], dst_ref=c_in.at[x],
-            send_sem=c_send.at[m], recv_sem=c_recv.at[x],
+            send_sem=c_send.at[slot(x, m)], recv_sem=c_recv.at[slot(m, x)],
             device_id={"sp": z * nx + m}, device_id_type=MESH)
 
     def forward_spread():
@@ -408,7 +420,7 @@
         c = h * nx + m
         held = b_in[m, 4 * h : 4 * h + 4].reshape(dvx, DK).astype(BF16)
         at = pl.ds(pl.multiple_of(c * wide, wide), wide)
-        value = (vp_buf[:, at] + nt(k_span[:, hd(h)], held)).astype(BF16)
+        value = (vp_buf[:, at] + nt(ksp_buf[:, hd(h)], held)).astype(BF16)
         vg_buf[c] = value
         vx_out[c] = value.astype(F32)
         near_copy(c).start()
@@ -440,6 +452,7 @@
 
     @pl.when(z < nz - 1)
     def _():
+        value_side()
         local_side()
 
     if cube:
@@ -447,6 +460,10 @@
         def _():
             x_relay(0)
 
+        @pl.when(z < nz - 2)
+        def _():
+            x_relay(1)
+
     if not cube:
         @pl.when(z < nz - 2)
         def _():
@@ -455,12 +472,17 @@
     if cube:
         @pl.when(z < nz - 2)
         def _():
-            x_relay(1)
+            for p in range(2, x_parts):
+                x_relay(p)
 
         @pl.when(z == 0)
         def _():
             scatter_wait(0)
             forward_step()
+
+    @pl.when(z == nz - 1)
+    def _():
+        value_side(0, 1)
 
     half_v = dvx // 4
 
@@ -508,16 +530,19 @@
             def _():
                 b_in[m, c] = b_out[m, c]
 
-        if cube and c % 4 == 3:
+        if cube and c == 3:
             @pl.when((z < nz - 1) & (z % 2 == 0))
             def _():
-                emit(h, x)
+                emit(0, x)
+
+            @pl.when(z == 0)
+            def _():
+                x_forward()
 
     if cube:
         @pl.when((z < nz - 1) & (z % 2 == 1))
         def _():
-            for h in range(heads):
-                emit(h, x)
+            emit(0, x)
     else:
         @pl.when(z == nz - 2)
         def _():
@@ -526,12 +551,16 @@
     @pl.when(z == nz - 1)
     def _():
         if cube:
-            x_send(1)
+            for p in range(1, x_parts):
+                x_send(p)
+            x_relay(0)
+        value_side(1, heads)
+        if cube:
+            x_relay(1)
         local_side()
         if cube:
-            x_relay(0)
-            for h in range(heads):
-                emit(h, x)
+            for p in range(2, x_parts):
+                x_relay(p)
         else:
             scatter_wait(0)
 
@@ -539,15 +568,18 @@
         lax.fori_loop(0, blocks, state_step, 0)
 
     if cube:
-        state_loop()
-
-        @pl.when(z < nz - 2)
+        @pl.when(z < nz - 1)
+        def _():
+            state_loop()
+
+        @pl.when((z > 0) & (z < nz - 2))
         def _():
             x_forward()
 
-        @pl.when(z >= nz - 2)
-        def _():
-            x_relay(1)
+        @pl.when(z == nz - 2)
+        def _():
+            for p in range(1, x_parts - 1):
+                x_relay(p)
 
         for h in range(heads):
             for c in range(4 * h, 4 * (h + 1)):
@@ -555,9 +587,28 @@
                     src_ref=b_out.at[1 - x, c], dst_ref=b_in.at[1 - x, c],
                     send_sem=b_send.at[1 - x], recv_sem=b_recv.at[0, c],
                     device_id={"sp": z * nx + 1 - x}, device_id_type=MESH).wait_recv()
-            emit(h, 1 - x)
+
+            @pl.when(z < nz - 1)
+            def _():
+                emit(h, 1 - x)
+                if h == 0:
+                    emit(1, x)
+
+                    @pl.when(z == nz - 2)
+                    def _():
+                        x_relay(x_parts - 1)
+
+            @pl.when(z == nz - 1)
+            def _():
+                for m in range(nx):
+                    emit(h, m)
+
             for m in range(nx):
                 fr_buf[h, m * dvx : (m + 1) * dvx, :] = b_in[m, 4 * h : 4 * h + 4].reshape(dvx, DK)
+
+        @pl.when(z == nz - 1)
+        def _():
+            state_loop()
     else:
         for h in range(heads):
             for m in range(nx):
@@ -571,7 +622,7 @@
                     at = m * dvx + c % 4 * half_v
                     fr_buf[h, at : at + half_v, :] = b_in[m, c]
             narrow = fr_buf[h].astype(BF16)
-            vg_buf[:, hv(h)] = (vp_buf[:, hv(h)] + nt(k_span[:, hd(h)], narrow)).astype(BF16)
+            vg_buf[:, hv(h)] = (vp_buf[:, hv(h)] + nt(ksp_buf[:, hd(h)], narrow)).astype(BF16)
 
 
     half_c = cols // 2
@@ -605,7 +656,7 @@
             k_grad = (
                 tail_buf[:, hd(h)] * kp_buf[:, hd(h)]
                 + jnp.exp(-c_buf[:, hd(h)]) * tn(dots, qg_buf[:, hd(h)])
-                + k_far[:, hd(h)] * nn(v_buf[:, hv(h)], fr_buf[h].astype(BF16))
+                + jnp.exp(total(h) - span_buf[:, hd(h)]) * nn(v_buf[:, hv(h)], fr_buf[h].astype(BF16))
             )
             kp_buf[:, hd(h)] = k_grad
             dk_ref[:, hd(h)] = k_grad.astype(BF16)
@@ -623,7 +674,7 @@
             def _():
                 pltpu.make_async_remote_copy(
                     src_ref=c_out.at[m], dst_ref=c_in.at[m],
-                    send_sem=c_send.at[m], recv_sem=c_recv.at[m],
+                    send_sem=c_send.at[slot(x, m)], recv_sem=c_recv.at[slot(x, m)],
                     device_id={"sp": z * nx + m}, device_id_type=MESH).wait_recv()
         upper = jnp.where(col >= row, 1.0, 0.0).astype(BF16)
         for h in range(first_head, last_head):
@@ -685,53 +736,73 @@
             scatter_wait(0)
             forward_step()
 
-        k0, k1, k2, k3 = x, nx + x, 1 - x, nx + 1 - x
+        late_half = z >= nz - 2
+        turns = [jnp.where(late_half, i, (i // nx) * nx + (x if i % nx == 0 else 1 - x)) for i in range(chunks)]
+        s0, s1, s2, s3 = turns
+        f0, f1, f2, f3 = [jnp.where(late_half, turns[i], turns[i ^ 1]) for i in range(chunks)]
         x_take()
-        take_near(k0)
-        side_send(k0, 0)
-        take_near(k1)
-        side_send(k1, 0)
-        key_side()
-        take_near(k2)
-        side_send(k2, 0)
-
-        @pl.when(z == nz - 2)
-        def _():
+        take_near(s0)
+        side_send(s0, 0)
+
+        @pl.when(z < nz - 1)
+        def _():
+            keep(s0, 0)
+            key_side()
+            take_near(s1)
+            side_send(s1, 0)
+            keep(s1, 0)
+            far_send(f0)
+            take_near(s2)
+            side_send(s2, 0)
+
+            @pl.when(z == nz - 2)
+            def _():
+                scatter_wait(0)
+                forward_step()
+
+            take_near(s3)
+            side_send(s3, 0)
+            far_send(f1)
+            side_send(s0, 1)
+            side_send(s1, 1)
+            keep(s2, 0)
+            keep(s3, 0)
+            far_send(f2)
+            side_send(s2, 1)
+            side_send(s3, 1)
+            far_send(f3)
+            for c in range(chunks):
+                keep(c, 1)
+
+        @pl.when(z == nz - 1)
+        def _():
+            for c in (s1, s2, s3):
+                take_near(c)
+                side_send(c, 0)
+            key_side()
+            for c in range(chunks):
+                keep(c, 0)
+                side_send(c, 1)
+                keep(c, 1)
+            far_send(0)
+            far_copy(1 - x, 0).wait_recv()
+            for c in range(1, chunks):
+                far_send(c)
             scatter_wait(0)
             forward_step()
 
-        keep(k2, 0)
-        far_send(k2)
-        side_send(k0, 1)
-        take_near(k3)
-        side_send(k3, 0)
-        keep(k3, 0)
-        far_send(k3)
-        side_send(k1, 1)
-        keep(k0, 0)
-        keep(k1, 0)
-
-        side_send(k2, 1)
-        far_send(k0)
-        side_send(k3, 1)
-
-        @pl.when(z == nz - 1)
-        def _():
-            scatter_wait(0)
-            forward_step()
-
-        keep(k2, 1)
-        keep(k3, 1)
-        far_send(k1)
-        keep(k0, 1)
-        keep(k1, 1)
         query_side(0, heads)
         squares = [0.0, 0.0]
-        for c in (k2, k3, k0, k1):
-            at = pl.ds(pl.multiple_of(c * wide, wide), wide)
+        for c in range(chunks):
+            at = slice(c * wide, (c + 1) * wide)
             for u in range(2):
                 side_copy(c, 1, u).wait_recv()
-                far_copy(c, u).wait_recv()
+                if c < nx and u == 0:
+                    @pl.when((z < nz - 1) | (c != 1 - x))
+                    def _():
+                        far_copy(c, u).wait_recv()
+                else:
+                    far_copy(c, u).wait_recv()
                 done = acc_buf[c, 1, u] + sx_in[c, 1, u] + sm_in[c, u]
                 dw_ref[u * half_r : (u + 1) * half_r, at] = done
                 squares[u] = squares[u] + done * done
@@ -741,7 +812,7 @@
     def norm_copy(off):
         return pltpu.make_async_remote_copy(
             src_ref=norm_out, dst_ref=norm_in.at[off],
-            send_sem=n_send.at[off], recv_sem=n_recv.at[off],
+            send_sem=n_send, recv_sem=n_recv.at[off - 1],
             device_id={"tp": (mine + off) % ntp}, device_id_type=MESH)
 
     for off in range(1, ntp):
@@ -801,17 +872,20 @@
 
     norms = norm_out[...]
     for off in range(1, ntp):
-        norm_copy(off).wait()
+        norm_copy(off).wait_recv()
         norms = norms + norm_in[off]
-    rn_ref[...] = norms
+    rn_ref[...] = norms[:, :1]
+    pltpu.make_async_remote_copy(
+        src_ref=norm_in.at[pl.ds(1, ntp - 1)], dst_ref=norm_in.at[pl.ds(1, ntp - 1)],
+        send_sem=n_send, recv_sem=n_recv.at[0],
+        device_id={"tp": (mine + 1) % ntp}, device_id_type=MESH).wait_send()
 
 
 def finish(*refs):
     sems = refs[10]
-    writes = [pltpu.make_async_copy(refs[i], refs[5 + i], sems.at[i]) for i in range(4)]
+    writes = [pltpu.make_async_copy(refs[i], refs[5 + i], sems.at[i]) for i in range(5)]
     for write in writes:
         write.start()
-    refs[9][...] = refs[4][:, :1]
     for write in writes:
         write.wait()
 
@@ -838,8 +912,8 @@
     cube = is_cube(n, nx, ntp) and cols == 2 * DV
     if cube:
         late = [
-            vm((2, half, tokens), F32),
-            vm((ntp, 2, half, tokens), F32),
+            vm((4, own // 4, tokens), F32),
+            vm((ntp, 4, own // 4, tokens), F32),
             vm((ntp, own, tokens), BF16),
             vm((chunks, tokens, wide_c), F32),
             vm((chunks, tokens, wide_c), F32),
@@ -850,7 +924,8 @@
             vm((chunks, 2, half, wide_c), F32),
             vm((chunks, 2, half, wide_c), F32),
             dma((4,)),
-            dma((ntp, 2)),
+            dma((8,)),
+            dma((2,)),
             dma,
             dma((chunks,)),
             dma,
@@ -865,7 +940,7 @@
             vm((tokens, wide), BF16),
             vm((tokens, wide), F32),
             vm((own, cols), F32),
-            vm((2, 8, own // 2), F32),
+            vm((2, 1, own // 2), F32),
         ),
         in_specs=[pl.BlockSpec(memory_space=pltpu.HBM)] * 6,
         out_specs=(pl.BlockSpec(memory_space=vm),) * 5,
@@ -906,17 +981,18 @@
             dma((2, nx)),
             dma((nx - 1,)),
             dma((nx - 1, 4 * heads)),
-            dma((nz,)),
-            dma((nz,)),
-            dma((nx,)),
-            dma((nx,)),
+            dma((1 if cube else nz,)),
+            dma((1 if cube else nz,)),
+            dma((nx - 1,)),
+            dma((nx - 1,)),
             dma,
             dma((4 * heads,)),
             dma((nx,)),
             dma((nx - 1, 4 * heads)),
-            dma((ntp,)),
-            dma((ntp,)),
+            dma,
+            dma((ntp - 1,)),
             vm((tokens, wide), F32),
+            vm((tokens, wide), BF16),
             *late,
         ],
         compiler_params=pltpu.CompilerParams(
@@ -928,8 +1004,8 @@
         out_shape=tuple(jax.ShapeDtypeStruct(a.shape, a.dtype) for a in out[:4])
         + (jax.ShapeDtypeStruct((2, 1, own // 2), F32),),
         in_specs=[pl.BlockSpec(memory_space=vm)] * 5,
-        out_specs=(pl.BlockSpec(memory_space=pltpu.HBM),) * 4 + (pl.BlockSpec(memory_space=vm),),
-        scratch_shapes=[dma((4,))],
+        out_specs=(pl.BlockSpec(memory_space=pltpu.HBM),) * 5,
+        scratch_shapes=[dma((5,))],
         compiler_params=pltpu.CompilerParams(vmem_limit_bytes=1024 * 1024),
     )(*out)
     return (*final[:4], final[4].reshape(-1))

time: 55.3 us -> 53.7 us (0.971)
  the two profiles are of different devices: /device:TPU:0 before, /device:TPU:17 now
where the time goes in v5:
time: 53.7 us; the launch traced here: 53.6 us
  Pallas kernels  52.9 us (99%)
  between operations  0.64 us (1%)
    pallas_call x1, Pallas kernels, on_device(): pl.pallas_call(functools.partial(kernel, n, nx, ntp), out_shape=(vm((toke...  51.9 us

profile of v5, /device:TPU:17, one launch (start us, length us, event | category | flops | bytes accessed | tf_op | source)
XLA Modules:
  0.0 53.6 jit_solution(13604978571460808245)
XLA Ops:
  0.6 51.9 %shard_map.101 = (bf16[256,256]{1,0:T(8,128)(2,1)S(1)}, bf16[256,256]{1,0:T(8,128)(2,1)S(1)}, f32[256,256]{1,0:T(8,128)S(1)}, f32[256,512]{1,0:T(8,128)S(1)}, f32[2,1,128]{2,1,0:T(1,128)S(1)}) custom-call(bf16[256,2048]{1,0:T(8,128)(2,1)} %x_hbm.1, bf16[256,256]{1,0:T(8,128)(2,1)} %q_hbm.1, bf16[256,256]{1,0:T(8,128)(2,1)} %k_hbm.1, ...), custom_call_target="tpu_custom_call" | custom-call | tf_op jit(solution)/shard_map/pallas_call | solution.py:936
  52.6 1.0 %shard_map.102 = (bf16[256,256]{1,0:T(8,128)(2,1)}, bf16[256,256]{1,0:T(8,128)(2,1)}, f32[256,256]{1,0:T(8,128)}, f32[256,512]{1,0:T(8,128)}, f32[2,1,128]{2,1,0:T(1,128)}) custom-call(bf16[256,256]{1,0:T(8,128)(2,1)S(1)} %get-tuple-element.15.refs_0_, bf16[256,256]{1,0:T(8,128)(2,1)S(1)} %get-tuple-element.16.refs_1_, ...), custom_call_target="tpu_custom_call" | custom-call | tf_op jit(solution)/shard_map/pallas_call | solution.py:1002

commit v6 on v5

--- a/solution.py
+++ b/solution.py
@@ -85,7 +85,7 @@
             [(g_hbm, g_ref), (q_hbm, q_ref), (o_hbm, o_ref), (k_hbm, k_ref), (x_hbm, x_ref), (w_hbm, w_ref)]
         )
     ]
-    for load in loads:
+    for load in loads[:3]:
         load.start()
     barrier = pltpu.get_barrier_semaphore()
     for off in range(1, nx):
@@ -169,6 +169,8 @@
                 a_in[d, m, h] = a_out[d, m, h]
 
     loads[0].wait()
+    for i in (4, 5, 3):
+        loads[i].start()
     for h in range(heads):
         span = sum(nn(tri, part_) for part_ in pieces(g_ref[:, hd(h)], 3))
         span_buf[:, hd(h)] = span
@@ -498,7 +500,35 @@
             send_sem=b_send.at[m], recv_sem=b_recv.at[slot(m, x), c],
             device_id={"sp": z * nx + m}, device_id_type=MESH)
 
+    late_half = z >= nz - 2
+    turns = [
+        jnp.where(late_half, i, (i // nx) * nx + (x if i % nx == 0 else 1 - x)) for i in range(2 * nx)]
+    s0, s1, s2, s3 = turns if cube else (0, 0, 0, 0)
+
+    def open_side():
+        x_take()
+        take_near(s0)
+        side_send(s0, 0)
+
+    def other_slice(h):
+        for c in range(4 * h, 4 * (h + 1)):
+            pltpu.make_async_remote_copy(
+                src_ref=b_out.at[1 - x, c], dst_ref=b_in.at[1 - x, c],
+                send_sem=b_send.at[1 - x], recv_sem=b_recv.at[0, c],
+                device_id={"sp": z * nx + 1 - x}, device_id_type=MESH).wait_recv()
+
     for c in range(4 * heads):
+        if cube and c == 4:
+            @pl.when(z == 0)
+            def _():
+                open_side()
+
+        if cube and c == 6:
+            @pl.when(z == 0)
+            def _():
+                other_slice(0)
+                emit(0, 1 - x)
+
         h, rows_ = c // 4, slice(8 + c % 4 * half_v, 8 + (c % 4 + 1) * half_v)
         first_wait(h, c % 4)
         acc, dec = composite(1, h, rows_)
@@ -531,7 +561,7 @@
                 b_in[m, c] = b_out[m, c]
 
         if cube and c == 3:
-            @pl.when((z < nz - 1) & (z % 2 == 0))
+            @pl.when(z < nz - 1)
             def _():
                 emit(0, x)
 
@@ -540,9 +570,9 @@
                 x_forward()
 
     if cube:
-        @pl.when((z < nz - 1) & (z % 2 == 1))
-        def _():
-            emit(0, x)
+        @pl.when(z == 0)
+        def _():
+            emit(1, x)
     else:
         @pl.when(z == nz - 2)
         def _():
@@ -581,30 +611,32 @@
             for p in range(1, x_parts - 1):
                 x_relay(p)
 
-        for h in range(heads):
-            for c in range(4 * h, 4 * (h + 1)):
-                pltpu.make_async_remote_copy(
-                    src_ref=b_out.at[1 - x, c], dst_ref=b_in.at[1 - x, c],
-                    send_sem=b_send.at[1 - x], recv_sem=b_recv.at[0, c],
-                    device_id={"sp": z * nx + 1 - x}, device_id_type=MESH).wait_recv()
-
-            @pl.when(z < nz - 1)
-            def _():
-                emit(h, 1 - x)
-                if h == 0:
-                    emit(1, x)
-
-                    @pl.when(z == nz - 2)
-                    def _():
-                        x_relay(x_parts - 1)
-
-            @pl.when(z == nz - 1)
-            def _():
+        def keep_pieces():
+            for h in range(heads):
+                for m in range(nx):
+                    fr_buf[h, m * dvx : (m + 1) * dvx, :] = b_in[m, 4 * h : 4 * h + 4].reshape(dvx, DK)
+
+        @pl.when((z > 0) & (z < nz - 1))
+        def _():
+            other_slice(0)
+            emit(0, 1 - x)
+            emit(1, x)
+
+            @pl.when(z == nz - 2)
+            def _():
+                x_relay(x_parts - 1)
+
+            other_slice(1)
+            emit(1, 1 - x)
+            keep_pieces()
+
+        @pl.when(z == nz - 1)
+        def _():
+            for h in range(heads):
+                other_slice(h)
                 for m in range(nx):
                     emit(h, m)
-
-            for m in range(nx):
-                fr_buf[h, m * dvx : (m + 1) * dvx, :] = b_in[m, 4 * h : 4 * h + 4].reshape(dvx, DK)
+            keep_pieces()
 
         @pl.when(z == nz - 1)
         def _():
@@ -736,22 +768,31 @@
             scatter_wait(0)
             forward_step()
 
-        late_half = z >= nz - 2
-        turns = [jnp.where(late_half, i, (i // nx) * nx + (x if i % nx == 0 else 1 - x)) for i in range(chunks)]
-        s0, s1, s2, s3 = turns
         f0, f1, f2, f3 = [jnp.where(late_half, turns[i], turns[i ^ 1]) for i in range(chunks)]
-        x_take()
-        take_near(s0)
-        side_send(s0, 0)
+        @pl.when(z > 0)
+        def _():
+            open_side()
 
         @pl.when(z < nz - 1)
         def _():
             keep(s0, 0)
-            key_side()
+
+            @pl.when(z > 0)
+            def _():
+                key_side()
+
             take_near(s1)
             side_send(s1, 0)
             keep(s1, 0)
             far_send(f0)
+
+            @pl.when(z == 0)
+            def _():
+                other_slice(1)
+                emit(1, 1 - x)
+                keep_pieces()
+                key_side()
+
             take_near(s2)
             side_send(s2, 0)
 

time: 53.7 us -> 53 us (0.987)
  Pallas kernels: 52.9 us -> 52.1 us
    pallas_call x1, Pallas kernels: 51.9 us -> 51.1 us  [on_device(): pl.pallas_call(functools.partial(kernel, n, nx, ntp), out_shape=(vm((toke...]
where the time goes in v6:
time: 53 us; the launch traced here: 52.8 us
  Pallas kernels  52.1 us (98%)
  between operations  0.64 us (1%)
    pallas_call x1, Pallas kernels, on_device(): pl.pallas_call(functools.partial(kernel, n, nx, ntp), out_shape=(vm((toke...  51.1 us

profile of v6, /device:TPU:17, one launch (start us, length us, event | category | flops | bytes accessed | tf_op | source)
XLA Modules:
  0.0 52.8 jit_solution(13911264035484515562)
XLA Ops:
  0.6 51.1 %shard_map.101 = (bf16[256,256]{1,0:T(8,128)(2,1)S(1)}, bf16[256,256]{1,0:T(8,128)(2,1)S(1)}, f32[256,256]{1,0:T(8,128)S(1)}, f32[256,512]{1,0:T(8,128)S(1)}, f32[2,1,128]{2,1,0:T(1,128)S(1)}) custom-call(bf16[256,2048]{1,0:T(8,128)(2,1)} %x_hbm.1, bf16[256,256]{1,0:T(8,128)(2,1)} %q_hbm.1, bf16[256,256]{1,0:T(8,128)(2,1)} %k_hbm.1, ...), custom_call_target="tpu_custom_call" | custom-call | tf_op jit(solution)/shard_map/pallas_call | solution.py:977
  51.7 1.0 %shard_map.102 = (bf16[256,256]{1,0:T(8,128)(2,1)}, bf16[256,256]{1,0:T(8,128)(2,1)}, f32[256,256]{1,0:T(8,128)}, f32[256,512]{1,0:T(8,128)}, f32[2,1,128]{2,1,0:T(1,128)}) custom-call(bf16[256,256]{1,0:T(8,128)(2,1)S(1)} %get-tuple-element.15.refs_0_, bf16[256,256]{1,0:T(8,128)(2,1)S(1)} %get-tuple-element.16.refs_1_, ...), custom_call_target="tpu_custom_call" | custom-call | tf_op jit(solution)/shard_map/pallas_call | solution.py:1043

commit v7 on v6

--- a/solution.py
+++ b/solution.py
@@ -68,7 +68,7 @@
     cube = is_cube(n, nx, ntp) and dw_ref.shape[1] == 2 * DV
     if cube:
         (xs_out, xr_in, xr_buf, vx_out, vx_in, vgp_buf, sx_out, sx_in, acc_buf, sm_out, sm_in,
-         xs_send, xr_recv, xc_recv, v_send, v_recv, sx_send, sx_recv, sm_send, sm_recv) = late
+         xs_send, xr_recv, xc_recv, v_send, v_recv, sx_send, sx_recv, sb_recv, sm_send, sm_recv) = late
     else:
         first, part, ring, r_send, r_recv = late
     nz = n // nx
@@ -206,19 +206,20 @@
 
     def x_copy(p):
         return pltpu.make_async_remote_copy(
-            src_ref=xs_out.at[p], dst_ref=xr_in.at[mine, p],
+            src_ref=xs_out.at[p], dst_ref=xr_in.at[p, mine],
             send_sem=xs_send.at[0], recv_sem=xr_recv.at[4 + p],
             device_id={"sp": near * nx + x}, device_id_type=MESH)
 
-    def x_pass(which, block, p, mate):
-        return pltpu.make_async_remote_copy(
-            src_ref=xr_in.at[block, p], dst_ref=xr_in.at[block, p],
-            send_sem=xs_send.at[which], recv_sem=xr_recv.at[p] if which == 2 else xc_recv.at[which // 2],
+    def x_pass(which, quart, p, mate):
+        return pltpu.make_async_remote_copy(
+            src_ref=xr_in.at[p, quart], dst_ref=xr_in.at[p, quart],
+            send_sem=xs_send.at[which],
+            recv_sem=xr_recv.at[p] if which == 2 else xc_recv.at[which // 2, p // nx],
             device_id={"tp": mate}, device_id_type=MESH)
 
     def x_send(p):
-        slab = jnp.where(mine < nx, nz - 1 - near, near)
-        xs_out[p] = xt_buf[block_rows(slab, mine % nx, p * x_rows, x_rows), :].astype(F32)
+        slab = nz - 1 - near if p < nx else near
+        xs_out[p] = xt_buf[block_rows(slab, p % nx, mine * x_rows, x_rows), :].astype(F32)
         x_copy(p).start()
 
     def x_relay(p):
@@ -226,19 +227,18 @@
         x_pass(2, mine, p, row_mate).start()
         x_pass(1, mine, p, core_mate).start()
 
-    def x_forward():
-        for p in range(x_parts):
+    def x_forward(first_part=0, last_part=4):
+        for p in range(first_part, last_part):
             x_pass(2, row_mate, p, row_mate).wait_recv()
             x_pass(3, row_mate, p, core_mate).start()
 
-    def x_take():
-        far_mate = (core_mate + 2) % 4
-        for i, block in enumerate((core_mate, far_mate)):
+    def x_take(part):
+        for i in range(2):
             pltpu.make_async_remote_copy(
-                src_ref=xr_in.at[block], dst_ref=xr_in.at[block],
-                send_sem=xs_send.at[1], recv_sem=xc_recv.at[i],
+                src_ref=xr_in.at[nx * part, pl.ds(0, nx)], dst_ref=xr_in.at[nx * part, pl.ds(0, nx)],
+                send_sem=xs_send.at[1], recv_sem=xc_recv.at[i, part],
                 device_id={"tp": core_mate}, device_id_type=MESH).wait_recv()
-        for j in range(2 * nx):
+        for j in range(nx * part, nx * (part + 1)):
             for p in range(x_parts):
                 xr_buf[j, p * x_rows : (p + 1) * x_rows] = xr_in[j, p].astype(BF16)
 
@@ -409,13 +409,13 @@
     def side_copy(c, s, u):
         return pltpu.make_async_remote_copy(
             src_ref=sx_out.at[c, s, u], dst_ref=sx_in.at[c, s, u],
-            send_sem=sx_send, recv_sem=sx_recv.at[c, s, u],
+            send_sem=sx_send, recv_sem=sx_recv.at[c, u] if s == 0 else sb_recv,
             device_id={"sp": z * nx + 1 - x}, device_id_type=MESH)
 
     def far_copy(c, u):
         return pltpu.make_async_remote_copy(
             src_ref=sm_out.at[c, u], dst_ref=sm_in.at[c, u],
-            send_sem=sm_send, recv_sem=sm_recv.at[c, u],
+            send_sem=sm_send, recv_sem=sm_recv.at[c],
             device_id={"sp": mirror * nx + x}, device_id_type=MESH)
 
     def emit(h, m):
@@ -427,6 +427,12 @@
         vx_out[c] = value.astype(F32)
         near_copy(c).start()
 
+    def far_take(c):
+        pltpu.make_async_remote_copy(
+            src_ref=sm_in.at[c], dst_ref=sm_in.at[c],
+            send_sem=sm_send, recv_sem=sm_recv.at[c],
+            device_id={"sp": mirror * nx + x}, device_id_type=MESH).wait_recv()
+
     def piece(c, s, xx):
         slab = mirror if s == 0 else z
         return nn(xt_buf[block_rows(slab, xx), :], vg_buf[c]) + nn(xr_buf[s * nx + xx], vgp_buf[c])
@@ -497,7 +503,7 @@
     def piece_copy(m, c):
         return pltpu.make_async_remote_copy(
             src_ref=b_out.at[m, c], dst_ref=b_in.at[x, c],
-            send_sem=b_send.at[m], recv_sem=b_recv.at[slot(m, x), c],
+            send_sem=b_send.at[m], recv_sem=b_recv.at[slot(m, x), c // 4],
             device_id={"sp": z * nx + m}, device_id_type=MESH)
 
     late_half = z >= nz - 2
@@ -506,16 +512,16 @@
     s0, s1, s2, s3 = turns if cube else (0, 0, 0, 0)
 
     def open_side():
-        x_take()
+        x_take(0)
         take_near(s0)
         side_send(s0, 0)
 
     def other_slice(h):
-        for c in range(4 * h, 4 * (h + 1)):
-            pltpu.make_async_remote_copy(
-                src_ref=b_out.at[1 - x, c], dst_ref=b_in.at[1 - x, c],
-                send_sem=b_send.at[1 - x], recv_sem=b_recv.at[0, c],
-                device_id={"sp": z * nx + 1 - x}, device_id_type=MESH).wait_recv()
+        part = pl.ds(4 * h, 4)
+        pltpu.make_async_remote_copy(
+            src_ref=b_out.at[1 - x, part], dst_ref=b_in.at[1 - x, part],
+            send_sem=b_send.at[1 - x], recv_sem=b_recv.at[0, h],
+            device_id={"sp": z * nx + 1 - x}, device_id_type=MESH).wait_recv()
 
     for c in range(4 * heads):
         if cube and c == 4:
@@ -644,15 +650,13 @@
     else:
         for h in range(heads):
             for m in range(nx):
-                for c in range(4 * h, 4 * (h + 1)):
-                    @pl.when(m != x)
-                    def _():
-                        pltpu.make_async_remote_copy(
-                            src_ref=b_out.at[m, c], dst_ref=b_in.at[m, c],
-                            send_sem=b_send.at[m], recv_sem=b_recv.at[slot(x, m), c],
-                            device_id={"sp": z * nx + m}, device_id_type=MESH).wait_recv()
-                    at = m * dvx + c % 4 * half_v
-                    fr_buf[h, at : at + half_v, :] = b_in[m, c]
+                @pl.when(m != x)
+                def _():
+                    pltpu.make_async_remote_copy(
+                        src_ref=b_out.at[m, pl.ds(4 * h, 4)], dst_ref=b_in.at[m, pl.ds(4 * h, 4)],
+                        send_sem=b_send.at[m], recv_sem=b_recv.at[slot(x, m), h],
+                        device_id={"sp": z * nx + m}, device_id_type=MESH).wait_recv()
+                fr_buf[h, m * dvx : (m + 1) * dvx, :] = b_in[m, 4 * h : 4 * h + 4].reshape(dvx, DK)
             narrow = fr_buf[h].astype(BF16)
             vg_buf[:, hv(h)] = (vp_buf[:, hv(h)] + nt(ksp_buf[:, hd(h)], narrow)).astype(BF16)
 
@@ -761,7 +765,7 @@
     else:
         @pl.when(z >= nz - 2)
         def _():
-            x_forward()
+            x_forward(0, 2)
 
         @pl.when((z > 0) & (z < nz - 2))
         def _():
@@ -793,6 +797,10 @@
                 keep_pieces()
                 key_side()
 
+            @pl.when(z == nz - 2)
+            def _():
+                x_forward(2, 4)
+
             take_near(s2)
             side_send(s2, 0)
 
@@ -804,6 +812,7 @@
             take_near(s3)
             side_send(s3, 0)
             far_send(f1)
+            x_take(1)
             side_send(s0, 1)
             side_send(s1, 1)
             keep(s2, 0)
@@ -820,13 +829,15 @@
             for c in (s1, s2, s3):
                 take_near(c)
                 side_send(c, 0)
+            x_forward(2, 4)
             key_side()
+            x_take(1)
             for c in range(chunks):
                 keep(c, 0)
                 side_send(c, 1)
                 keep(c, 1)
             far_send(0)
-            far_copy(1 - x, 0).wait_recv()
+            far_take(1 - x)
             for c in range(1, chunks):
                 far_send(c)
             scatter_wait(0)
@@ -834,16 +845,18 @@
 
         query_side(0, heads)
         squares = [0.0, 0.0]
+        pltpu.make_async_remote_copy(
+            src_ref=sm_in, dst_ref=sm_in, send_sem=sx_send, recv_sem=sb_recv,
+            device_id={"sp": z * nx + 1 - x}, device_id_type=MESH).wait_recv()
         for c in range(chunks):
             at = slice(c * wide, (c + 1) * wide)
+            if c < nx:
+                @pl.when((z < nz - 1) | (c != 1 - x))
+                def _():
+                    far_take(c)
+            else:
+                far_take(c)
             for u in range(2):
-                side_copy(c, 1, u).wait_recv()
-                if c < nx and u == 0:
-                    @pl.when((z < nz - 1) | (c != 1 - x))
-                    def _():
-                        far_copy(c, u).wait_recv()
-                else:
-                    far_copy(c, u).wait_recv()
                 done = acc_buf[c, 1, u] + sx_in[c, 1, u] + sm_in[c, u]
                 dw_ref[u * half_r : (u + 1) * half_r, at] = done
                 squares[u] = squares[u] + done * done
@@ -904,9 +917,9 @@
                 device_id={"sp": near * nx + x}, device_id_type=MESH).wait_send()
 
         all_sent(xs_out, xs_send.at[0])
-        all_sent(xr_in.at[mine], xs_send.at[1])
-        all_sent(xr_in.at[mine], xs_send.at[2])
-        all_sent(xr_in.at[row_mate], xs_send.at[3])
+        all_sent(xr_in.at[0], xs_send.at[1])
+        all_sent(xr_in.at[0], xs_send.at[2])
+        all_sent(xr_in.at[0], xs_send.at[3])
         all_sent(vx_out, v_send)
         all_sent(sx_out, sx_send)
         all_sent(sm_out, sm_send)
@@ -966,13 +979,14 @@
             vm((chunks, 2, half, wide_c), F32),
             dma((4,)),
             dma((8,)),
-            dma((2,)),
+            dma((2, 2)),
             dma,
             dma((chunks,)),
             dma,
-            dma((chunks, 2, 2)),
+            dma((chunks, 2)),
             dma,
-            dma((chunks, 2)),
+            dma,
+            dma((chunks,)),
         ]
     out = pl.pallas_call(
         functools.partial(kernel, n, nx, ntp),
@@ -1029,7 +1043,7 @@
             dma,
             dma((4 * heads,)),
             dma((nx,)),
-            dma((nx - 1, 4 * heads)),
+            dma((nx - 1, heads)),
             dma,
             dma((ntp - 1,)),
             vm((tokens, wide), F32),

time: 53 us -> 52.6 us (level)
  no operation moved by 1% of the time
where the time goes in v7:
time: 52.6 us; the launch traced here: 52.5 us
  Pallas kernels  51.8 us (98%)
  between operations  0.64 us (1%)
    pallas_call x1, Pallas kernels, on_device(): pl.pallas_call(functools.partial(kernel, n, nx, ntp), out_shape=(vm((toke...  50.8 us

profile of v7, /device:TPU:17, one launch (start us, length us, event | category | flops | bytes accessed | tf_op | source)
XLA Modules:
  0.0 52.5 jit_solution(5984560821246698162)
XLA Ops:
  0.6 50.8 %shard_map.101 = (bf16[256,256]{1,0:T(8,128)(2,1)S(1)}, bf16[256,256]{1,0:T(8,128)(2,1)S(1)}, f32[256,256]{1,0:T(8,128)S(1)}, f32[256,512]{1,0:T(8,128)S(1)}, f32[2,1,128]{2,1,0:T(1,128)S(1)}) custom-call(bf16[256,2048]{1,0:T(8,128)(2,1)} %x_hbm.1, bf16[256,256]{1,0:T(8,128)(2,1)} %q_hbm.1, bf16[256,256]{1,0:T(8,128)(2,1)} %k_hbm.1, ...), custom_call_target="tpu_custom_call" | custom-call | tf_op jit(solution)/shard_map/pallas_call | solution.py:991
  51.5 1.0 %shard_map.102 = (bf16[256,256]{1,0:T(8,128)(2,1)}, bf16[256,256]{1,0:T(8,128)(2,1)}, f32[256,256]{1,0:T(8,128)}, f32[256,512]{1,0:T(8,128)}, f32[2,1,128]{2,1,0:T(1,128)}) custom-call(bf16[256,256]{1,0:T(8,128)(2,1)S(1)} %get-tuple-element.15.refs_0_, bf16[256,256]{1,0:T(8,128)(2,1)S(1)} %get-tuple-element.16.refs_1_, ...), custom_call_target="tpu_custom_call" | custom-call | tf_op jit(solution)/shard_map/pallas_call | solution.py:1057

commit v8 on v7

--- a/solution.py
+++ b/solution.py
@@ -761,7 +761,7 @@
                 dw_ref[u * half_r : (u + 1) * half_r, d * half_c : (d + 1) * half_c] = done
                 for at in range(0, half_c, 128):
                     squares = squares + done[:, at : at + 128] * done[:, at : at + 128]
-            norm_out[u] = jnp.broadcast_to(jnp.sum(squares.T, axis=0, keepdims=True), (8, half_r))
+            norm_out[u : u + 1, :] = jnp.sum(squares.T, axis=0, keepdims=True)
     else:
         @pl.when(z >= nz - 2)
         def _():
@@ -861,7 +861,7 @@
                 dw_ref[u * half_r : (u + 1) * half_r, at] = done
                 squares[u] = squares[u] + done * done
         for u in range(2):
-            norm_out[u] = jnp.broadcast_to(jnp.sum(squares[u].T, axis=0, keepdims=True), (8, half_r))
+            norm_out[u : u + 1, :] = jnp.sum(squares[u].T, axis=0, keepdims=True)
 
     def norm_copy(off):
         return pltpu.make_async_remote_copy(
@@ -928,7 +928,8 @@
     for off in range(1, ntp):
         norm_copy(off).wait_recv()
         norms = norms + norm_in[off]
-    rn_ref[...] = norms[:, :1]
+    for u in range(2):
+        rn_ref[u] = norms[u : u + 1]
     pltpu.make_async_remote_copy(
         src_ref=norm_in.at[pl.ds(1, ntp - 1)], dst_ref=norm_in.at[pl.ds(1, ntp - 1)],
         send_sem=n_send, recv_sem=n_recv.at[0],
@@ -1031,8 +1032,8 @@
             vm((nx, 4 * heads, dvx // 4, DK), F32),
             vm((nx, 4 * heads, dvx // 4, DK), F32),
             vm((heads, DV, DK), F32),
-            vm((2, 8, own // 2), F32),
-            vm((ntp, 2, 8, own // 2), F32),
+            vm((2, own // 2), F32),
+            vm((ntp, 2, own // 2), F32),
             dma((2, nx)),
             dma((nx - 1,)),
             dma((nx - 1, 4 * heads)),

time: 52.6 us -> 52.5 us (level)
  no operation moved by 1% of the time
where the time goes in v8:
time: 52.5 us; the launch traced here: 52.4 us
  Pallas kernels  51.8 us (99%)
  between operations  0.64 us (1%)
    pallas_call x1, Pallas kernels, on_device(): pl.pallas_call(functools.partial(kernel, n, nx, ntp), out_shape=(vm((toke...  50.7 us

profile of v8, /device:TPU:17, one launch (start us, length us, event | category | flops | bytes accessed | tf_op | source)
XLA Modules:
  0.0 52.4 jit_solution(11210085522318326240)
XLA Ops:
  0.6 50.7 %shard_map.101 = (bf16[256,256]{1,0:T(8,128)(2,1)S(1)}, bf16[256,256]{1,0:T(8,128)(2,1)S(1)}, f32[256,256]{1,0:T(8,128)S(1)}, f32[256,512]{1,0:T(8,128)S(1)}, f32[2,1,128]{2,1,0:T(1,128)S(1)}) custom-call(bf16[256,2048]{1,0:T(8,128)(2,1)} %x_hbm.1, bf16[256,256]{1,0:T(8,128)(2,1)} %q_hbm.1, bf16[256,256]{1,0:T(8,128)(2,1)} %k_hbm.1, ...), custom_call_target="tpu_custom_call" | custom-call | tf_op jit(solution)/shard_map/pallas_call | solution.py:992
  51.4 1.0 %shard_map.102 = (bf16[256,256]{1,0:T(8,128)(2,1)}, bf16[256,256]{1,0:T(8,128)(2,1)}, f32[256,256]{1,0:T(8,128)}, f32[256,512]{1,0:T(8,128)}, f32[2,1,128]{2,1,0:T(1,128)}) custom-call(bf16[256,256]{1,0:T(8,128)(2,1)S(1)} %get-tuple-element.15.refs_0_, bf16[256,256]{1,0:T(8,128)(2,1)S(1)} %get-tuple-element.16.refs_1_, ...), custom_call_target="tpu_custom_call" | custom-call | tf_op jit(solution)/shard_map/pallas_call | solution.py:1058
